TPU v7x, 256 devices: a 4x2x16 block of a 4x16x16 slice. The times are simulated.
256 devices in a mesh: grp: 2 (over y), fs: 16 (over z), tp: 8 (over x, core).
Axes of the slice: x: 4, y: 2, z: 16, core: 2. Of those that a mesh axis runs over, the one named last changes fastest.
The devices are a block of a 4x16x16 slice.
Arguments:
- tokens: bfloat16 [16384, 2048], P(('grp', 'fs'), 'tp'), parts along dimension 0, may hold values from -36 to 36
- query_matrix: bfloat16 [2048, 1024], P('fs', 'tp'), may hold values from -0.125 to 0.125
- key_weight: bfloat16 [2048, 1024], P('fs', 'tp'), may hold values from -0.125 to 0.125
- value_weight: bfloat16 [2048, 2048], P('fs', 'tp'), may hold values from -0.125 to 0.125
- forget_lower_factor: bfloat16 [2048, 32], replicated, may hold values from -0.125 to 0.125
- decay_up: bfloat16 [32, 1024], replicated, may hold values from -1 to 1
- decay_bias: float32 [1024], replicated, may hold values from -1 to 8
- log_extra: float32 [16384, 1024], P(('grp', 'fs'), 'tp'), parts along dimension 0, may hold values from -0.7 to 0
- head_gain: float32 [256], replicated, may hold values from 0.1 to 1.9
- out_weight: bfloat16 [2048, 2048], P('tp', 'fs'), may hold values from -0.125 to 0.125
- mix_gain: float32 [2048], P('tp'), may hold values from 0.1 to 1.9
- up_weight: bfloat16 [2048, 8192], P('fs', 'tp'), may hold values from -0.125 to 0.125
- down_weight: bfloat16 [8192, 2048], P('tp', 'fs'), may hold values from -0.0625 to 0.0625
- out_gain: float32 [2048], P('tp'), may hold values from 0.1 to 1.9
Outputs:
- layer_out: bfloat16 [16384, 2048], P(('grp', 'fs'), 'tp'), parts along dimension 0
There are 2 independent parts, one for each index of `grp`. A program takes and returns all parts, laid end to end along the dimension named above; an argument that names none is the same for every part. Nothing has to cross between parts.
All inputs are finite; a program needn't handle non-finite values.
Results may differ from a plain program's by a relative error of at most 0.015.
Values may be sent and summed in bfloat16 or wider, within the bound.
A program may use at most 64 MiB of HBM per device.

v0:
```python
import jax
import jax.numpy as jnp
from jax import lax
from jax.sharding import PartitionSpec as P

D = 2048
DK = 128
DV = 256
SEGMENT_LENGTH = 64


ALPHA = 2.0**0.5
TAU = 16.0
EPS = 1e-05


def copy_for_each(x, axis):
    copies = jnp.broadcast_to(x, (lax.axis_size(axis), *x.shape))
    return lax.all_to_all(copies, axis, split_axis=0, concat_axis=0, tiled=True)


def of_everyone(x, axis):
    everything = copy_for_each(x, axis)
    return jnp.sum(everything, axis=0)


def in_one(arrays, axis):
    ends = [0]
    for a in arrays:
        ends.append(ends[-1] + a.size)
    subtotal = of_everyone(jnp.concatenate([a.ravel() for a in arrays]), axis)
    return tuple((subtotal[b:e].reshape(a.shape) for a, b, e in zip(arrays, ends, ends[1:])))


def in_order(tiles, dim):
    lengths = list(tiles.shape[1:])
    lengths[dim] *= tiles.shape[0]
    return jnp.moveaxis(tiles, 0, dim).reshape(lengths)


def gather_directly(x, axis, dim):
    return in_order(copy_for_each(x, axis), dim)


def side_by_side(arrays, axis, dim, along):
    both = jnp.concatenate(arrays, axis=along)
    out, at, finished = (lax.all_gather(both, axis, axis=dim, tiled=True), 0, [])
    for a in arrays:
        finished.append(lax.slice_in_dim(out, at, at + a.shape[along], axis=along))
        at += a.shape[along]
    return tuple(finished)


def cut_along(x, dim, devices):
    lengths = x.shape
    tiles = x.reshape(*lengths[:dim], devices, lengths[dim] // devices, *lengths[dim + 1 :])
    return jnp.moveaxis(tiles, dim, 0)


def summed_on_arrival(x, axis, dim):
    devices = lax.axis_size(axis)
    tiles = lax.all_to_all(cut_along(x, dim, devices), axis, 0, 0, tiled=True)
    return jnp.sum(tiles.astype(jnp.float32), axis=0)


def turned_gather(arrays, axis, dims):
    turned = [jnp.moveaxis(a, dim, 0) for a, dim in zip(arrays, dims)]
    widths = [t[0].size for t in turned]
    both = jnp.concatenate([t.reshape(-1, w) for t, w in zip(turned, widths)], axis=1)
    out = lax.all_gather(both, axis, axis=0, tiled=True)
    tiles = jnp.split(out, [sum(widths[:k]) for k in range(1, len(widths))], axis=1)
    return tuple(
        (
            jnp.moveaxis(b.reshape(-1, *t.shape[1:]), 0, dim)
            for b, t, dim in zip(tiles, turned, dims)
        )
    )


def block_scan(queries, key_rows, value_rows, log_decay):
    span = queries.shape[2]
    causal = (jnp.arange(span)[:, None] >= jnp.arange(span)[None, :])[:, :, None]

    def step(state, inputs):
        query_block, key_block, value_block, decay_block = inputs
        cumul = jnp.cumsum(decay_block, axis=1)
        last_cum = cumul[:, -1:, :]
        carried = jnp.einsum("hcd,hde->hce", query_block * jnp.exp(cumul), state)
        differ = cumul[:, :, None, :] - cumul[:, None, :, :]
        weights = jnp.exp(jnp.where(causal, differ, -jnp.inf))
        scores = jnp.sum(query_block[:, :, None, :] * key_block[:, None, :, :] * weights, axis=-1)
        within = jnp.einsum("hij,hje->hie", scores, value_block)
        fresh = jnp.einsum("hcd,hce->hde", key_block * jnp.exp(last_cum - cumul), value_block)
        new_state = jnp.exp(last_cum[:, 0, :])[:, :, None] * state + fresh
        return (new_state, carried + within)

    start = jnp.zeros((queries.shape[1], queries.shape[3], value_rows.shape[3]), jnp.float32)
    _, outputs = lax.scan(step, start, (queries, key_rows, value_rows, log_decay))
    return outputs


def layer_norm(summed, gain_cols):
    row_total, row_squares = in_one(
        (jnp.sum(summed, axis=1), jnp.sum(summed * summed, axis=1)), "tp"
    )
    row_mean = row_total / D
    row_var = row_squares / D - row_mean * row_mean
    centered = summed - row_mean[:, None]
    return (centered * lax.rsqrt(row_var[:, None] + EPS) * gain_cols).astype(jnp.bfloat16)


def local(
    tokens,
    query_matrix,
    key_weight,
    value_weight,
    forget_lower_factor,
    decay_up,
    decay_bias,
    log_extra,
    head_gain,
    out_weight,
    mix_gain,
    up_weight,
    down_weight,
    out_gain,
):
    gathered = gather_directly(tokens, "tp", 1)
    row_count = gathered.shape[0]
    key_cols = query_matrix.shape[1]
    value_cols = value_weight.shape[1]
    local_heads = key_cols // DK
    block_pieces = side_by_side((query_matrix, key_weight, value_weight), "fs", 0, 1)
    queries, key_rows, value_rows = tuple(
        (
            jnp.dot(gathered, shard_piece, preferred_element_type=jnp.float32)
            for shard_piece in block_pieces
        )
    )
    queries = queries.astype(jnp.bfloat16)
    key_rows = key_rows.astype(jnp.bfloat16)
    value_rows = value_rows.astype(jnp.bfloat16)
    low = jnp.dot(gathered, forget_lower_factor, preferred_element_type=jnp.float32).astype(
        jnp.bfloat16
    )
    offset_cols = lax.axis_index("tp") * key_cols
    local_up = lax.dynamic_slice_in_dim(decay_up, offset_cols, key_cols, 1)
    local_bias = lax.dynamic_slice_in_dim(decay_bias, offset_cols, key_cols, 0)
    gate_pre = jnp.dot(low, local_up, preferred_element_type=jnp.float32) + local_bias
    log_decay = jax.nn.log_sigmoid(gate_pre) / TAU + log_extra
    count = row_count // SEGMENT_LENGTH

    def blocks(array, depth):
        return (
            array.astype(jnp.float32)
            .reshape(count, SEGMENT_LENGTH, local_heads, depth)
            .transpose(0, 2, 1, 3)
        )

    attended = block_scan(
        blocks(queries, DK) * DK ** (-0.5),
        blocks(key_rows, DK),
        blocks(value_rows, DV),
        blocks(log_decay, DK),
    )
    attended = attended.transpose(0, 2, 1, 3).reshape(row_count, local_heads, DV)
    scaled = (
        attended
        * lax.rsqrt(jnp.mean(attended * attended, axis=-1, keepdims=True) + EPS)
        * head_gain
    )
    mixed_heads = scaled.reshape(row_count, value_cols).astype(jnp.bfloat16)
    mix_terms = jnp.dot(
        mixed_heads, gather_directly(out_weight, "fs", 1), preferred_element_type=jnp.float32
    )
    mix = summed_on_arrival(mix_terms.astype(jnp.bfloat16), "tp", 1)
    normed_local = layer_norm(ALPHA * tokens.astype(jnp.float32) + mix, mix_gain)
    normed_rows = gather_directly(normed_local, "tp", 1)
    up_whole, down_whole = turned_gather((up_weight, down_weight), "fs", (0, 1))
    hidden = jnp.dot(normed_rows, up_whole, preferred_element_type=jnp.float32)
    activation = jnp.square(jax.nn.relu(hidden)).astype(jnp.bfloat16)
    down_terms = jnp.dot(activation, down_whole, preferred_element_type=jnp.float32)
    down = summed_on_arrival(down_terms.astype(jnp.bfloat16), "tp", 1)
    return layer_norm(ALPHA * normed_local.astype(jnp.float32) + down, out_gain)


def solution(mesh):
    in_specs = (
        P(("grp", "fs"), "tp"),
        P("fs", "tp"),
        P("fs", "tp"),
        P("fs", "tp"),
        P(),
        P(),
        P(),
        P(("grp", "fs"), "tp"),
        P(),
        P("tp", "fs"),
        P("tp"),
        P("fs", "tp"),
        P("tp", "fs"),
        P("tp"),
    )
    out_specs = P(("grp", "fs"), "tp")
    return jax.shard_map(local, mesh=mesh, in_specs=in_specs, out_specs=out_specs, check_vma=False)
```

profile of v0, /device:TPU:33, one launch (start us, length us, event | category | flops | bytes accessed | tf_op | source)
XLA Modules:
  0.0 320.4 jit_solution(16596478524238506429)
XLA Ops:
  6.6 1.6 pad_maximum_fusion.1
  10.8 24.1 %all-to-all-start = ((bf16[8,512,256]{1,2,0:T(8,128)(2,1)}), bf16[8,512,256]{1,2,0:T(8,128)(2,1)S(1)}, u32[]{:S(2)}, u32[]{:S(2)}) async-start(bf16[8,512,256]{1,2,0:T(8,128)(2,1)} %broadcast_in_dim.58), calls=%async_computation | async-start | bytes 4194304 | tf_op jit(solution)/shard_map/all_to_all | solution.py:19
  36.9 24.3 %all-to-all-done = bf16[8,512,256]{1,2,0:T(8,128)(2,1)S(1)} async-done(((bf16[8,512,256]{1,2,0:T(8,128)(2,1)}), bf16[8,512,256]{1,2,0:T(8,128)(2,1)S(1)}, u32[]{:S(2)}, u32[]{:S(2)}) %all-to-all-start) | async-done | bytes 2097184 | tf_op jit(solution)/shard_map/all_to_all | solution.py:19
  62.2 5.7 %all-to-all-start.1 = ((bf16[16,256,128]{1,2,0:T(8,128)(2,1)}), bf16[16,256,128]{1,2,0:T(8,128)(2,1)S(1)}, u32[]{:S(2)}, u32[]{:S(2)}) async-start(bf16[16,256,128]{1,2,0:T(8,128)(2,1)} %broadcast_in_dim.59), calls=%async_computation.1 | async-start | bytes 2097152 | tf_op jit(solution)/shard_map/all_to_all | solution.py:19
  67.9 2.5 fusion.57
  70.3 45.0 %all-gather.3.cloned.1.call-done = bf16[2048,512]{1,0:T(8,128)(2,1)} async-done(((bf16[128,512]{1,0:T(8,128)(2,1)}), bf16[2048,512]{1,0:T(8,128)(2,1)}) %all-gather.3.cloned.1.call-update) | async-done | bytes 2097168 | tf_op jit(solution)/shard_map/all_gather | solution.py:47
  115.4 2.6 fusion.42
  118.0 1.8 copy.59
  119.8 2.2 fusion.46
  122.0 1.8 copy.60
  123.8 2.2 fusion.48
  127.1 51.2 %while.13 = (s32[]{:T(128)}, f32[1,128,256]{2,1,0:T(8,128)S(1)}, f32[8,1,64,256]{3,2,1,0:T(8,128)}, f32[8,1,64,128]{3,2,1,0:T(8,128)}, f32[8,1,64,128]{3,2,1,0:T...) while((s32[]{:T(128)}, f32[1,128,256]{2,1,0:T(8,128)S(1)}, ...), condition=%wide.region_3.4_spmd.clone, body=%wide.region_0.3_spmd.clone.sunk | while | flops 13795331 | bytes 1177212 | solution.py:98
  131.0 1.5 fusion.94
  143.8 1.5 fusion.94
  169.4 1.5 fusion.94
  175.8 1.5 fusion.94
  179.6 1.8 convolution_convert_fusion
  181.6 42.0 %all_to_all.37 = bf16[8,512,256]{2,1,0:T(8,128)(2,1)S(1)} all-to-all(bf16[8,512,256]{2,1,0:T(8,128)(2,1)S(1)} %bitcast.141), channel_id=1, replica_groups=mesh['grp'=2,'fs'=16,'tp'=8] {'tp'}, dimensions={0} | all-to-all | bytes 4194304 | tf_op jit(solution)/shard_map/all_to_all | solution.py:62
  224.8 8.2 %all_to_all.38 = f32[8,1,1024]{2,1,0:T(1,128)S(1)} all-to-all(f32[8,1,1024]{2,1,0:T(1,128)S(1)} %broadcast_in_dim.60), channel_id=1, replica_groups=mesh['grp'=2,'fs'=16,'tp'=8] {'tp'}, dimensions={0} | all-to-all | bytes 65536 | tf_op jit(solution)/shard_map/all_to_all | solution.py:19
  233.6 29.4 %all_to_all.39 = bf16[8,512,256]{1,2,0:T(8,128)(2,1)S(1)} all-to-all(bf16[8,512,256]{1,2,0:T(8,128)(2,1)S(1)} %broadcast_in_dim.61), channel_id=1, replica_groups=mesh['grp'=2,'fs'=16,'tp'=8] {'tp'}, dimensions={0} | all-to-all | bytes 4194304 | tf_op jit(solution)/shard_map/all_to_all | solution.py:19
  262.9 9.4 %fusion.34 = bf16[512,2048]{1,0:T(8,128)(2,1)} fusion(bf16[2048,2048]{0,1:T(8,128)(2,1)} %all-gather.5.cloned.1.call-done, bf16[512,2048]{0,1:T(8,128)(2,1)S(1)} %bitcast.145), kind=kOutput, calls=%fused_computation.43 | convolution fusion | flops 4297588736 | bytes 12582912 | tf_op jit(solution)/shard_map/dot_general | solution.py:182
  272.4 1.7 copy.82
  274.1 29.7 %all_to_all.40 = bf16[8,512,256]{2,1,0:T(8,128)(2,1)S(1)} all-to-all(bf16[8,512,256]{2,1,0:T(8,128)(2,1)S(1)} %bitcast.142), channel_id=1, replica_groups=mesh['grp'=2,'fs'=16,'tp'=8] {'tp'}, dimensions={0} | all-to-all | bytes 4194304 | tf_op jit(solution)/shard_map/all_to_all | solution.py:62
  304.4 8.2 %all_to_all.41 = f32[8,1,1024]{2,1,0:T(1,128)S(1)} all-to-all(f32[8,1,1024]{2,1,0:T(1,128)S(1)} %broadcast_in_dim.62), channel_id=1, replica_groups=mesh['grp'=2,'fs'=16,'tp'=8] {'tp'}, dimensions={0} | all-to-all | bytes 65536 | tf_op jit(solution)/shard_map/all_to_all | solution.py:19
  (128 shorter events, 56.3 us)
Async XLA Ops:
  6.5 61.3 %copy-start = (bf16[2048,32]{0,1:T(8,128)(2,1)S(1)}, bf16[2048,32]{0,1:T(8,128)(2,1)}, u32[]{:S(2)}) copy-start(bf16[2048,32]{0,1:T(8,128)(2,1)} %param.20) | copy-start | bytes 393220
  6.6 108.8 %all-gather.3.cloned.1.call-start = ((), (), s32[]{:S(2)}) async-start(), calls=%async_computation.7 | async-start | bytes 2228224 | tf_op jit(solution)/shard_map/all_gather | solution.py:47
  10.8 24.1 %copy-start.2 = (bf16[128,1024]{1,0:T(8,128)(2,1)S(1)}, bf16[128,1024]{1,0:T(8,128)(2,1)}, u32[]{:S(2)}) copy-start(bf16[128,1024]{1,0:T(8,128)(2,1)} %param.27) | copy-start | bytes 786436
  10.8 24.2 %copy-start.3 = (bf16[1024,128]{1,0:T(8,128)(2,1)S(1)}, bf16[1024,128]{1,0:T(8,128)(2,1)}, u32[]{:S(2)}) copy-start(bf16[1024,128]{1,0:T(8,128)(2,1)} %param.28) | copy-start | bytes 786436
  10.8 50.4 %all-to-all-start = ((bf16[8,512,256]{1,2,0:T(8,128)(2,1)}), bf16[8,512,256]{1,2,0:T(8,128)(2,1)S(1)}, u32[]{:S(2)}, u32[]{:S(2)}) async-start(bf16[8,512,256]{1,2,0:T(8,128)(2,1)} %broadcast_in_dim.58), calls=%async_computation | async-start | bytes 4194304 | tf_op jit(solution)/shard_map/all_to_all | solution.py:19
  34.8 1.1 copy-start.4
  34.8 228.1 %all-gather.5.cloned.1.call-start = ((), (), s32[]{:S(2)}) async-start(), calls=%async_computation.8 | async-start | bytes 8912896 | tf_op jit(solution)/shard_map/all_gather | solution.py:70
  62.2 117.4 %all-to-all-start.1 = ((bf16[16,256,128]{1,2,0:T(8,128)(2,1)}), bf16[16,256,128]{1,2,0:T(8,128)(2,1)S(1)}, u32[]{:S(2)}, u32[]{:S(2)}) async-start(bf16[16,256,128]{1,2,0:T(8,128)(2,1)} %broadcast_in_dim.59), calls=%async_computation.1 | async-start | bytes 2097152 | tf_op jit(solution)/shard_map/all_to_all | solution.py:19
  127.1 52.6 %copy-start.7 = (f32[256]{0:T(256)S(1)}, f32[256]{0:T(256)}, u32[]{:S(2)}) copy-start(f32[256]{0:T(256)} %param.24) | copy-start | bytes 3076
  223.6 1.0 copy-start.1
  223.6 9.5 %copy-start.5 = (f32[256]{0:T(256)S(1)}, f32[256]{0:T(256)}, u32[]{:S(2)}) copy-start(f32[256]{0:T(256)} %param.26) | copy-start | bytes 3076
  303.8 8.8 %copy-start.6 = (f32[256]{0:T(256)S(1)}, f32[256]{0:T(256)}, u32[]{:S(2)}) copy-start(f32[256]{0:T(256)} %param.29) | copy-start | bytes 3076
Sparse Core Ops, SparseCore 0:
  9.1 106.1 all-gather.2
  117.1 123.7 all-gather.4
where the time goes:
time: 324 us; the launch traced here: 320 us
  blocking collectives  117 us (36%)
  waiting for transfers between devices  69.4 us (21%)
  matrix products  47.8 us (15%)
  starting transfers between devices  29.7 us (9%)
  local copies, waits for them, and re-layouts  24.6 us (8%)
  other arithmetic  17.4 us (5%)
  between operations  13.7 us (4%)
    all_to_all x2, blocking collectives, summed_on_arrival(): tiles = lax.all_to_all(cut_along(x, dim, devices), axis, 0, 0, tiled=True)  71.7 us
    all_to_all x3, blocking collectives, copy_for_each(): return lax.all_to_all(copies, axis, split_axis=0, concat_axis=0, tiled=True)  45.7 us
    all_gather x1, waiting for transfers between devices, side_by_side(): lax.all_gather(both, axis, axis=dim, tiled=True)  45 us
    all_to_all x2, starting transfers between devices, copy_for_each(): return lax.all_to_all(copies, axis, split_axis=0, concat_axis=0, tiled=True)  29.7 us
    all_to_all x2, waiting for transfers between devices, copy_for_each(): return lax.all_to_all(copies, axis, split_axis=0, concat_axis=0, tiled=True)  24.3 us
    dot_general x8, matrix products, step(): within = jnp.einsum('hij,hje->hie', scores, value_block)  12.1 us
    reduce_sum x8, other arithmetic, step(): jnp.sum(query_block[:, :, None, :] * key_block[:, None, :, :] * weights,...  10.7 us
    dot_general x1, matrix products, local(): jnp.dot(activation, down_whole, preferred_element_type=jnp.float32)  9.41 us
  transfers between devices with their start and end apart: 4, of which 2 were waited for; matrix products, arithmetic and copies ran while one was open for 23% of the time, Pallas kernels for 0%

commit v1 on v0

v1 whole, which is shorter than its diff:
```python
import functools

import jax
import jax.numpy as jnp
import numpy as np
from jax import lax
from jax.experimental import pallas as pl
from jax.experimental.pallas import tpu as pltpu
from jax.sharding import PartitionSpec as P

DK = 128
DV = 256
TILE = 128
LEVELS = (64, 32, 16, 8, 4, 2, 1)
ALPHA = 2.0**0.5
TAU = 16.0
EPS = 1e-05
MESH = pl.DeviceIdType.MESH
BF = jnp.bfloat16
F32 = jnp.float32


def decay_sums():
    i = np.arange(TILE)[:, None]
    j = np.arange(TILE)[None, :]
    parts = []
    for m in LEVELS:
        mid = i // (2 * m) * (2 * m) + m - 1
        parts.append(np.where(i > mid, (j > mid) & (j <= i), (j > i) & (j <= mid)))
    parts.append(j <= i)
    parts.append(j > i)
    one = np.concatenate(parts, axis=0).astype(np.float32)
    return np.concatenate([one, one], axis=1)


def dot(a, b, dims=((1,), (0,))):
    return lax.dot_general(a, b, (dims, ((), ())), preferred_element_type=F32)


NT = ((1,), (1,))
TN = ((0,), (0,))


def kernel(
    n_fs,
    n_tp,
    tokens,
    q_w,
    k_w,
    v_w,
    o_w,
    up_w,
    dn_w,
    fl,
    d_up,
    d_bias,
    extra,
    h_gain,
    m_gain,
    o_gain,
    sums,
    out,
    tok,
    wqkv,
    wo,
    wup,
    wdn,
    esum,
    mixed,
    part1,
    part2,
    half_recv,
    fwd_recv,
    last_recv,
    fwd_send,
    last_send,
    nrm,
    act,
    own_out,
    out_buf,
    mg_all,
    og_all,
    local_sem,
    z_send,
    z_recv,
    y_send,
    y_recv,
    ag_send,
    ag_recv,
    rs_send,
    rs_recv,
    small_send,
    small_recv,
):
    z = lax.axis_index("fs")
    t = lax.axis_index("tp")
    grp = lax.axis_index("grp")
    g = lax.rem(grp, 2)
    mate = grp + 1 - 2 * g
    n_x = n_tp // 2
    x, c = t // 2, lax.rem(t, 2)
    right_t = 2 * lax.rem(x + 1, n_x) + c
    left_t = 2 * lax.rem(x + n_x - 1, n_x) + c
    across_t = 2 * lax.rem(x + 2, n_x) + c
    twin_t = t + 1 - 2 * c
    right_z = lax.rem(z + 1, n_fs)
    left_z = lax.rem(z + n_fs - 1, n_fs)
    rows = tok.shape[0]
    cols = tokens.shape[1]
    width = tok.shape[1]
    block = rows // n_tp
    zd = q_w.shape[0]

    def at(v, step):
        return pl.multiple_of(v * step, step)

    def remote(src, dst, ssem, rsem, dev):
        return pltpu.make_async_remote_copy(
            src_ref=src,
            dst_ref=dst,
            send_sem=ssem,
            recv_sem=rsem,
            device_id=dev,
            device_id_type=MESH,
        )

    pending = []

    def send(src, dst, ssem, rsem, dev):
        copy = remote(src, dst, ssem, rsem, dev)
        copy.start()
        pending.append(copy)

    def arrive(dst, ssem, rsem, dev):
        remote(dst, dst, ssem, rsem, dev).wait_recv()

    my_cols = pl.ds(at(z, zd), zd)
    kw = q_w.shape[1]
    vw = v_w.shape[1]
    own_rows = pl.ds(at(z, zd), zd)
    moves = [
        (q_w, wqkv.at[own_rows, pl.ds(0, kw)]),
        (k_w, wqkv.at[own_rows, pl.ds(kw, kw)]),
        (v_w, wqkv.at[own_rows, pl.ds(2 * kw, vw)]),
        (tokens, tok.at[:, pl.ds(at(t, cols), cols)]),
        (o_w, wo.at[:, my_cols]),
        (up_w, wup.at[own_rows, :]),
        (dn_w, wdn.at[:, my_cols]),
    ]
    moves = [pltpu.make_async_copy(s, d, local_sem.at[i]) for i, (s, d) in enumerate(moves)]
    for m in moves:
        m.start()

    barrier = pltpu.get_barrier_semaphore()
    peers = [{"fs": left_z}, {"fs": right_z}, {"grp": mate}]
    peers += [{"tp": lax.rem(t + k, n_tp)} for k in range(1, n_tp)]
    for p in peers:
        pl.semaphore_signal(barrier, inc=1, device_id=p, device_id_type=MESH)
    pl.semaphore_wait(barrier, len(peers))

    hq = zd // 2
    hu = zd // 4
    ho = wo.shape[0] // 2
    hd = wdn.shape[0] // 4

    def region(p, s, which):
        c0 = pl.ds(at(s, zd), zd)
        if p == 0:
            return wqkv.at[pl.ds(pl.multiple_of(s * zd + which * hq, hq), hq), :]
        if p == 1:
            return wo.at[pl.ds(at(which, ho), ho), c0]
        if p == 2:
            return wup.at[pl.ds(pl.multiple_of(s * zd + which * hu, hu), hu), :]
        if p == 3:
            return wdn.at[pl.ds(at(which, hd), hd), c0]
        if p in (4, 5):
            return wup.at[pl.ds(pl.multiple_of(s * zd + (p - 2) * hu, hu), hu), :]
        return wdn.at[pl.ds((p - 4) * hd, hd), c0]

    def whole(p):
        n = n_fs - 1
        if p == 0:
            return wqkv.at[pl.ds(0, n * hq), :]
        if p == 1:
            return wo.at[pl.ds(0, ho), pl.ds(0, n * zd)]
        if p in (2, 4, 5):
            return wup.at[pl.ds(0, n * hu), :]
        return wdn.at[pl.ds(0, hd), pl.ds(0, n * zd)]

    far = n_fs // 2
    near = n_fs - 1 - far
    reach = [(far, near) if p in (0, 2, 4, 6) else (near, far) for p in range(8)]

    def origin(d, h):
        return lax.rem(z + (n_fs - h if d == 0 else h), n_fs)

    def z_start(p, d, h):
        dev = {"fs": right_z if d == 0 else left_z}
        r = region(p, z if h == 1 else origin(d, h - 1), g)
        remote(r, r, z_send.at[p], z_recv.at[p, d, h - 1], dev).start()

    def z_event(p, d, h):
        dev = {"fs": left_z if d == 0 else right_z}
        arrive(region(p, origin(d, h), g), z_send.at[p], z_recv.at[p, d, h - 1], dev)
        if h < reach[p][d]:
            z_start(p, d, h + 1)

    def y_slot(d, h):
        return d * far + h - 1

    def y_start(p, d, h):
        r = region(p, origin(d, h), g)
        remote(r, r, y_send.at[p], y_recv.at[p, y_slot(d, h)], {"grp": mate}).start()

    def y_done(p):
        for d in range(2):
            for h in range(1, reach[p][d] + 1):
                r = region(p, origin(d, h), 1 - g)
                arrive(r, y_send.at[p], y_recv.at[p, y_slot(d, h)], {"grp": mate})

    first, second = (0, 1, 2), (3, 4, 6, 5, 7)
    order = []
    for h in range(1, far + 1):
        for p in first:
            for d in range(2):
                if h <= reach[p][d]:
                    order.append(functools.partial(z_event, p, d, h))
                    if p == 0:
                        order.append(functools.partial(y_start, p, d, h))
        if h == far - 1:
            for p in second:
                for d in range(2):
                    order.append(functools.partial(z_start, p, d, 1))
    split = len(order)
    for p in (1, 2):
        for h in range(1, far + 1):
            for d in range(2):
                if h <= reach[p][d]:
                    order.append(functools.partial(y_start, p, d, h))
    tail_from = len(order)
    for h in range(1, far + 1):
        for p in second:
            for d in range(2):
                if h <= reach[p][d]:
                    order.append(functools.partial(z_event, p, d, h))
                    if p == 3:
                        order.append(functools.partial(y_start, p, d, h))
    done = [0]

    def pump(upto):
        while done[0] < min(upto, len(order)):
            order[done[0]]()
            done[0] += 1

    def ease(n):
        pump(done[0] + n)

    def gather(i, view):
        ss, rs = ag_send.at[i], ag_recv.at[i]
        right, left, twin = {"tp": right_t}, {"tp": left_t}, {"tp": twin_t}

        def go(k, blk, half, dev):
            v = view(blk, half)
            send(v, v, ss.at[k], rs.at[k], dev)

        def got(k, blk, half, dev):
            arrive(view(blk, half), ss.at[k], rs.at[k], dev)

        def start():
            go(0, t, None, right)
            go(1, t, None, left)
            go(2, t, None, twin)

        def middle():
            got(0, left_t, None, left)
            go(3, left_t, 0, right)
            go(4, left_t, None, twin)
            got(1, right_t, None, right)
            go(5, right_t, 1, left)
            go(6, right_t, None, twin)

        def close():
            got(3, across_t, 0, left)
            go(7, across_t, 0, twin)
            got(5, across_t, 1, right)
            go(8, across_t, 1, twin)

        def finish():
            flip = 1 - 2 * c
            got(2, twin_t, None, twin)
            got(4, left_t + flip, None, twin)
            got(6, right_t + flip, None, twin)
            got(7, across_t + flip, 0, twin)
            got(8, across_t + flip, 1, twin)

        return start, middle, close, finish

    def tok_view(blk, half):
        r = pl.ds(0, rows) if half is None else pl.ds(half * (rows // 2), rows // 2)
        return tok.at[r, pl.ds(at(blk, cols), cols)]

    def nrm_view(blk, half):
        cc = pl.ds(0, width) if half is None else pl.ds(half * (width // 2), width // 2)
        return nrm.at[pl.ds(at(blk, block), block), cc]

    def scatter_sum(i, part):
        ss, rs = rs_send.at[i], rs_recv.at[i]
        right, left, twin = {"tp": right_t}, {"tp": left_t}, {"tp": twin_t}
        hw = width // 2

        for k in (2, 1, 3, 0):
            xx = lax.rem(x + k, n_x)
            send(
                part.at[pl.ds(at(2 * xx + 1 - c, block), block), :],
                half_recv.at[i, k],
                ss.at[k],
                rs.at[k],
                twin,
            )

        def pair(k):
            arrive(half_recv.at[i, k], ss.at[k], rs.at[k], twin)
            xx = lax.rem(x + k, n_x)
            mine = part[pl.ds(at(2 * xx + c, block), block), :]
            return mine.astype(F32) + half_recv[i, k].astype(F32)

        fwd_send[i] = pair(2).astype(BF)
        for k, (lo, dev) in enumerate(((0, right), (hw, left))):
            send(
                fwd_send.at[i, :, pl.ds(lo, hw)],
                fwd_recv.at[i, k],
                ss.at[4 + k],
                rs.at[4 + k],
                dev,
            )
        s1, s3 = pair(1), pair(3)
        last_send[i, 0, :, pl.ds(hw, hw)] = s1[:, hw:].astype(BF)
        last_send[i, 1, :, pl.ds(0, hw)] = s3[:, :hw].astype(BF)
        yield
        arrive(fwd_recv.at[i, 0], ss.at[4], rs.at[4], left)
        last_send[i, 0, :, pl.ds(0, hw)] = (s1[:, :hw] + fwd_recv[i, 0].astype(F32)).astype(BF)
        send(last_send.at[i, 0], last_recv.at[i, 0], ss.at[6], rs.at[6], right)
        arrive(fwd_recv.at[i, 1], ss.at[5], rs.at[5], right)
        last_send[i, 1, :, pl.ds(hw, hw)] = (s3[:, hw:] + fwd_recv[i, 1].astype(F32)).astype(BF)
        send(last_send.at[i, 1], last_recv.at[i, 1], ss.at[7], rs.at[7], left)
        total = pair(0)
        yield
        arrive(last_recv.at[i, 0], ss.at[6], rs.at[6], left)
        arrive(last_recv.at[i, 1], ss.at[7], rs.at[7], right)
        yield total + last_recv[i, 0].astype(F32) + last_recv[i, 1].astype(F32)

    def norm(v, gain):
        mean = jnp.mean(v, axis=1, keepdims=True)
        d = v - mean
        var = jnp.mean(d * d, axis=1, keepdims=True)
        return (d * lax.rsqrt(var + EPS) * gain).astype(BF)

    for i in (0, 1, 2):
        moves[i].wait()
    for d in range(2):
        z_start(0, d, 1)
    moves[3].wait()
    tok_start, tok_middle, tok_close, tok_finish = gather(0, tok_view)
    tok_start()
    for i in (4, 5, 6):
        moves[i].wait()
    for p in (1, 2):
        for d in range(2):
            z_start(p, d, 1)
    mine = pl.ds(at(t, cols), cols)
    for j, (src, dst) in enumerate(((m_gain, mg_all), (o_gain, og_all))):
        dst[:, mine] = src[...]
        for k in range(1, n_tp):
            send(
                src,
                dst.at[:, mine],
                small_send.at[j, k],
                small_recv.at[j, k],
                {"tp": lax.rem(t + k, n_tp)},
            )

    per_hop = 8
    pump(2 * per_hop)
    tok_middle()
    pump(3 * per_hop)
    tok_close()
    pump(4 * per_hop)
    tok_finish()

    key_cols = pl.ds(at(t, DK), DK)
    n_tiles = rows // TILE
    for i in range(n_tiles):
        rr = pl.ds(i * TILE, TILE)
        low = dot(tok[rr, :], fl[...]).astype(BF)
        pre = dot(low, d_up[:, key_cols]) + d_bias[:, key_cols]
        log_sig = jnp.minimum(pre, 0.0) - jnp.log1p(jnp.exp(-jnp.abs(pre)))
        decay = log_sig / TAU + extra[rr, :]
        hi = decay.astype(BF)
        lo = (decay - hi.astype(F32)).astype(BF)
        esum[i] = jnp.exp(dot(sums[...], jnp.concatenate([hi, lo], axis=0)))
        pump((5 + i) * per_hop)
    pump(tail_from)
    y_done(0)

    ii = lax.broadcasted_iota(jnp.int32, (TILE, TILE), 0)
    jj = lax.broadcasted_iota(jnp.int32, (TILE, TILE), 1)
    state = jnp.zeros((DV, DK), F32)
    n_lv = len(LEVELS)
    for i in range(n_tiles):
        rr = pl.ds(i * TILE, TILE)
        qkv = dot(tok[rr, :], wqkv[...]).astype(BF)
        ease(4)
        q = qkv[:, :DK].astype(F32) * DK**-0.5
        kb = qkv[:, DK : 2 * DK]
        k = kb.astype(F32)
        v = qkv[:, 2 * DK :]
        scores = jnp.where(ii == jj, dot(q.astype(BF), kb, NT), 0.0)
        for l, m in enumerate(LEVELS):
            e = esum[i, pl.ds(l * TILE, TILE), :]
            s = dot((q * e).astype(BF), (k * e).astype(BF), NT)
            scores = jnp.where(((ii ^ jj) // m == 1) & (ii > jj), s, scores)
        e_in = esum[i, pl.ds(n_lv * TILE, TILE), :]
        e_out = esum[i, pl.ds((n_lv + 1) * TILE, TILE), :]
        got = dot(scores.astype(BF), v)
        if i > 0:
            got = got + dot((q * e_in).astype(BF), state.astype(BF), NT)
        if i < n_tiles - 1:
            fresh = dot(v, (k * e_out).astype(BF), TN)
            state = state * e_in[TILE - 1 : TILE, :] + fresh
        scale = lax.rsqrt(jnp.mean(got * got, axis=1, keepdims=True) + EPS)
        mixed[rr, :] = (got * scale * h_gain[...]).astype(BF)
        ease(2)
    y_done(1)

    step = 256

    def mix_cols(j, _):
        cc = pl.ds(pl.multiple_of(j * step, step), step)
        part1[:, cc] = dot(mixed[...], wo[:, cc]).astype(BF)
        return 0

    lax.fori_loop(0, width // step, mix_cols, 0)
    rs1 = scatter_sum(0, part1)
    next(rs1)
    ease(6)
    next(rs1)
    ease(10)
    mix = next(rs1)
    for j, dst in enumerate((mg_all, og_all)):
        for k in range(1, n_tp):
            src_t = lax.rem(t + n_tp - k, n_tp)
            arrive(
                dst.at[:, pl.ds(at(src_t, cols), cols)],
                small_send.at[j, k],
                small_recv.at[j, k],
                {"tp": src_t},
            )
    my_rows = pl.ds(at(t, block), block)
    nrm[my_rows, :] = norm(ALPHA * tok[my_rows, :].astype(F32) + mix, mg_all[...])
    n_start, n_middle, n_close, n_finish = gather(1, nrm_view)
    n_start()
    ease(10)
    n_middle()
    ease(6)
    n_close()
    n_finish()
    pump(len(order))
    y_done(2)

    def up_cols(j, _):
        cc = pl.ds(pl.multiple_of(j * step, step), step)
        hidden = jnp.maximum(dot(nrm[...], wup[:, cc]), 0.0)
        act[:, cc] = (hidden * hidden).astype(BF)
        return 0

    lax.fori_loop(0, act.shape[1] // step, up_cols, 0)
    y_done(3)

    def down_cols(j, _):
        cc = pl.ds(pl.multiple_of(j * step, step), step)
        part2[:, cc] = dot(act[...], wdn[:, cc]).astype(BF)
        return 0

    lax.fori_loop(0, width // step, down_cols, 0)
    rs2 = scatter_sum(1, part2)
    next(rs2)
    next(rs2)
    down = next(rs2)
    own_out[...] = norm(ALPHA * nrm[my_rows, :].astype(F32) + down, og_all[...])
    out_buf[my_rows, :] = own_out[:, mine]
    for k in range(1, n_tp):
        dst_t = lax.rem(t + k, n_tp)
        send(
            own_out.at[:, pl.ds(at(dst_t, cols), cols)],
            out_buf.at[my_rows, :],
            small_send.at[2, k],
            small_recv.at[2, k],
            {"tp": dst_t},
        )
    for k in range(1, n_tp):
        src_t = lax.rem(t + n_tp - k, n_tp)
        arrive(
            out_buf.at[pl.ds(at(src_t, block), block), :],
            small_send.at[2, k],
            small_recv.at[2, k],
            {"tp": src_t},
        )
    out[...] = out_buf[...]
    for copy in pending:
        copy.wait_send()
    for p in range(8):
        w = whole(p)
        remote(w, w, z_send.at[p], z_recv.at[p, 0, 0], {"fs": right_z}).wait_send()
        if p < 4:
            remote(w, w, y_send.at[p], y_recv.at[p, 0], {"grp": mate}).wait_send()


def solution(mesh):
    n_fs, n_tp = mesh.shape["fs"], mesh.shape["tp"]
    assert n_tp == 8 and mesh.shape["grp"] % 2 == 0

    def local(
        tokens,
        query_matrix,
        key_weight,
        value_weight,
        forget_lower_factor,
        decay_up,
        decay_bias,
        log_extra,
        head_gain,
        out_weight,
        mix_gain,
        up_weight,
        down_weight,
        out_gain,
    ):
        rows, cols = tokens.shape
        width = cols * n_tp
        block = rows // n_tp
        zd = query_matrix.shape[0]
        hidden = up_weight.shape[1]
        vcols = value_weight.shape[1]
        qkv_cols = 2 * query_matrix.shape[1] + vcols
        sums = jnp.asarray(decay_sums(), BF)
        hbm = pl.BlockSpec(memory_space=pl.ANY)
        vmem = pl.BlockSpec(memory_space=pltpu.VMEM)
        far = n_fs // 2
        dma = pltpu.SemaphoreType.DMA
        return pl.pallas_call(
            functools.partial(kernel, n_fs, n_tp),
            out_shape=jax.ShapeDtypeStruct((rows, cols), BF),
            in_specs=[hbm] * 7 + [vmem] * 8,
            out_specs=vmem,
            scratch_shapes=[
                pltpu.VMEM((rows, width), BF),
                pltpu.VMEM((width, qkv_cols), BF),
                pltpu.VMEM((vcols, width), BF),
                pltpu.VMEM((width, hidden), BF),
                pltpu.VMEM((hidden, width), BF),
                pltpu.VMEM((rows // TILE, sums.shape[0], DK), F32),
                pltpu.VMEM((rows, vcols), BF),
                pltpu.VMEM((rows, width), BF),
                pltpu.VMEM((rows, width), BF),
                pltpu.VMEM((2, n_tp // 2, block, width), BF),
                pltpu.VMEM((2, 2, block, width // 2), BF),
                pltpu.VMEM((2, 2, block, width), BF),
                pltpu.VMEM((2, block, width), BF),
                pltpu.VMEM((2, 2, block, width), BF),
                pltpu.VMEM((rows, width), BF),
                pltpu.VMEM((rows, hidden), BF),
                pltpu.VMEM((block, width), BF),
                pltpu.VMEM((rows, cols), BF),
                pltpu.VMEM((1, width), F32),
                pltpu.VMEM((1, width), F32),
                dma((7,)),
                dma((8,)),
                dma((8, 2, far)),
                dma((4,)),
                dma((4, n_fs)),
                dma((2, 9)),
                dma((2, 9)),
                dma((2, 8)),
                dma((2, 8)),
                dma((3, n_tp)),
                dma((3, n_tp)),
            ],
            compiler_params=pltpu.CompilerParams(
                collective_id=0,
                has_side_effects=True,
                vmem_limit_bytes=60 * 1024 * 1024,
            ),
            name="layer",
        )(
            tokens,
            query_matrix,
            key_weight,
            value_weight,
            out_weight,
            up_weight,
            down_weight,
            forget_lower_factor,
            decay_up,
            decay_bias.reshape(1, -1),
            log_extra,
            head_gain.reshape(1, -1),
            mix_gain.reshape(1, -1),
            out_gain.reshape(1, -1),
            sums,
        )

    in_specs = (
        P(("grp", "fs"), "tp"),
        P("fs", "tp"),
        P("fs", "tp"),
        P("fs", "tp"),
        P(),
        P(),
        P(),
        P(("grp", "fs"), "tp"),
        P(),
        P("tp", "fs"),
        P("tp"),
        P("fs", "tp"),
        P("tp", "fs"),
        P("tp"),
    )
    out_specs = P(("grp", "fs"), "tp")
    return jax.shard_map(local, mesh=mesh, in_specs=in_specs, out_specs=out_specs, check_vma=False)
```

time: 324 us -> 152 us (0.47); the launches traced: 320 us -> 152 us
  Pallas kernels: 0 us -> 148 us
  blocking collectives: 117 us -> 0 us
  waiting for transfers between devices: 69.4 us -> 0 us
  matrix products: 47.8 us -> 0 us
  starting transfers between devices: 29.7 us -> 0 us
  local copies, waits for them, and re-layouts: 24.6 us -> 3.57 us
  other arithmetic: 17.4 us -> 0 us
  between operations: 13.7 us -> 0.01 us
    pallas_call x0 -> x1, Pallas kernels: none -> 148 us  [local(): pl.pallas_call(functools.partial(kernel, n_fs, n_tp), out_shape=jax.Shape...]
    all_to_all x5 -> x0, blocking collectives: 117 us -> none  [the longest x2 71.7 us: summed_on_arrival(): tiles = lax.all_to_all(cut_along(x, dim, devices), axis, 0, 0, tiled=True)]
    dot_general x30 -> x0, matrix products: 47.8 us -> none  [the longest x8 12.1 us: step(): within = jnp.einsum('hij,hje->hie', scores, value_block)]
    all_gather x2 -> x0, waiting for transfers between devices: 45 us -> none  [the longest x1 45 us: side_by_side(): lax.all_gather(both, axis, axis=dim, tiled=True)]
    all_to_all x2 -> x0, starting transfers between devices: 29.7 us -> none  [copy_for_each(): return lax.all_to_all(copies, axis, split_axis=0, concat_axis=0, tiled=True)]
    all_to_all x2 -> x0, waiting for transfers between devices: 24.3 us -> none  [copy_for_each(): return lax.all_to_all(copies, axis, split_axis=0, concat_axis=0, tiled=True)]
    reduce_sum x15 -> x0, other arithmetic: 13 us -> none  [the longest x8 10.7 us: step(): jnp.sum(query_block[:, :, None, :] * key_block[:, None, :, :] * weights,...]
    mul x9 -> x0, local copies, waits for them, and re-layouts: 7.92 us -> none  [the longest x8 6.15 us: step(): query_block[:, :, None, :] * key_block[:, None, :, :] * weights]
  transfers between devices with their start and end apart: 4 -> 0, of which waited for: 2 -> 0; matrix products, arithmetic and copies ran while one was open for 23% -> 0% of each run, Pallas kernels for 0% -> 0%
where the time goes in v1:
time: 152 us
  Pallas kernels  148 us (97%)
  local copies, waits for them, and re-layouts  3.57 us (2%)
    pallas_call x1, Pallas kernels, local(): pl.pallas_call(functools.partial(kernel, n_fs, n_tp), out_shape=jax.Shape...  148 us
    unnamed x2, local copies, waits for them, and re-layouts  3.57 us

profile of v1, /device:TPU:33, one launch (start us, length us, event | category | flops | bytes accessed | tf_op | source)
XLA Modules:
  0.0 152.0 jit_solution(17617692995884561734)
XLA Ops:
  0.0 1.9 %copy.16.fl = bf16[2048,32]{1,0:T(8,128)(2,1)} copy(bf16[2048,32]{0,1:T(8,128)(2,1)} %param.19) | data formatting | bytes 262144 | tf_op args[4]
  1.9 148.4 %layer.1 = bf16[512,256]{1,0:T(8,128)(2,1)} custom-call(bf16[512,256]{1,0:T(8,128)(2,1)} %tokens.1, bf16[128,128]{1,0:T(8,128)(2,1)} %q_w.1, bf16[128,128]{1,0:T(8,128)(2,1)} %k_w.1, bf16[128,256]{1,0:T(8,128)(2,1)} %v_w.1, bf16[256,128]{1,0:T(8,128)(2,1)} %o_w.1, bf16[128,1024]{1,0:T(8,128)(2,1)} %up_w.1, bf16[1024,128]{1,0:T(8,128)(2,1)} %dn_w.1, ...), custom_call_target="tpu_custom_call" | custom-call | tf_op jit(solution)/shard_map/layer/pallas_call | solution.py:550
  150.3 1.7 %copy.18 = bf16[512,256]{1,0:T(8,128)(2,1)} copy(bf16[512,256]{1,0:T(8,128)(2,1)} %layer.1) | data formatting | bytes 524288

commit v2 on v1

--- a/solution.py
+++ b/solution.py
@@ -39,6 +39,39 @@
 
 NT = ((1,), (1,))
 TN = ((0,), (0,))
+SIZES = (1.0, 0.5, 1.0, 1.0, 1.0, 1.0, 1.0, 1.0)
+RANKS = (0, 1, 2, 3, 2, 2, 3, 3)
+UNIT, DELAY, LEAD = 1.405, 2.0, 1.0
+RECV, Z_SEND, Y_SEND = 0, 1, 2
+ATTEND, MIXED, NORMED, UP_READY = 31.5, 40.0, 52.0, 64.0
+
+
+def ring_plan(reach, shared):
+    items, ready = [], []
+    for d in range(2):
+        waiting = [(0.0, p, 1) for p in range(len(reach))]
+        free = 0.0
+        while waiting:
+            now = max(free, min(w[0] for w in waiting))
+            best = min((w for w in waiting if w[0] <= now), key=lambda w: (RANKS[w[1]], w[0]))
+            waiting.remove(best)
+            since, p, h = best
+            items.append((max(now - LEAD, since), Z_SEND, p, d, h))
+            free = now + SIZES[p] * UNIT
+            items.append((free + DELAY, RECV, p, d, h))
+            if p < shared:
+                ready.append((free + DELAY, p, d, h))
+            if h < reach[p][d]:
+                waiting.append((free + DELAY, p, h + 1))
+    free = 0.0
+    while ready:
+        now = max(free, min(r[0] for r in ready))
+        best = min((r for r in ready if r[0] <= now), key=lambda r: (r[1], r[0]))
+        ready.remove(best)
+        since, p, d, h = best
+        items.append((max(now - LEAD, since), Y_SEND, p, d, h))
+        free = now + SIZES[p] * UNIT
+    return sorted(items)
 
 
 def kernel(
@@ -69,17 +102,20 @@
     mixed,
     part1,
     part2,
-    half_recv,
-    fwd_recv,
-    last_recv,
-    fwd_send,
-    last_send,
+    pair_row,
+    fwd_row_in,
+    last_row_in,
+    fwd_row_out,
+    last_row_out,
+    pair_col,
+    fwd_col_in,
+    last_col_in,
+    fwd_col_out,
+    last_col_out,
     nrm,
     act,
-    own_out,
-    out_buf,
+    stats,
     mg_all,
-    og_all,
     local_sem,
     z_send,
     z_recv,
@@ -202,8 +238,6 @@
     def z_event(p, d, h):
         dev = {"fs": left_z if d == 0 else right_z}
         arrive(region(p, origin(d, h), g), z_send.at[p], z_recv.at[p, d, h - 1], dev)
-        if h < reach[p][d]:
-            z_start(p, d, h + 1)
 
     def y_slot(d, h):
         return d * far + h - 1
@@ -218,42 +252,15 @@
                 r = region(p, origin(d, h), 1 - g)
                 arrive(r, y_send.at[p], y_recv.at[p, y_slot(d, h)], {"grp": mate})
 
-    first, second = (0, 1, 2), (3, 4, 6, 5, 7)
-    order = []
-    for h in range(1, far + 1):
-        for p in first:
-            for d in range(2):
-                if h <= reach[p][d]:
-                    order.append(functools.partial(z_event, p, d, h))
-                    if p == 0:
-                        order.append(functools.partial(y_start, p, d, h))
-        if h == far - 1:
-            for p in second:
-                for d in range(2):
-                    order.append(functools.partial(z_start, p, d, 1))
-    split = len(order)
-    for p in (1, 2):
-        for h in range(1, far + 1):
-            for d in range(2):
-                if h <= reach[p][d]:
-                    order.append(functools.partial(y_start, p, d, h))
-    tail_from = len(order)
-    for h in range(1, far + 1):
-        for p in second:
-            for d in range(2):
-                if h <= reach[p][d]:
-                    order.append(functools.partial(z_event, p, d, h))
-                    if p == 3:
-                        order.append(functools.partial(y_start, p, d, h))
+    steps = {RECV: z_event, Z_SEND: z_start, Y_SEND: y_start}
+    order = ring_plan(reach, 4)
     done = [0]
 
-    def pump(upto):
-        while done[0] < min(upto, len(order)):
-            order[done[0]]()
+    def pump(until):
+        while done[0] < len(order) and order[done[0]][0] <= until:
+            _, kind, p, d, h = order[done[0]]
+            steps[kind](p, d, h)
             done[0] += 1
-
-    def ease(n):
-        pump(done[0] + n)
 
     def gather(i, view):
         ss, rs = ag_send.at[i], ag_recv.at[i]
@@ -266,34 +273,41 @@
         def got(k, blk, half, dev):
             arrive(view(blk, half), ss.at[k], rs.at[k], dev)
 
+        flip = 1 - 2 * c
+
         def start():
-            go(0, t, None, right)
-            go(1, t, None, left)
-            go(2, t, None, twin)
-
-        def middle():
-            got(0, left_t, None, left)
-            go(3, left_t, 0, right)
-            go(4, left_t, None, twin)
-            got(1, right_t, None, right)
-            go(5, right_t, 1, left)
-            go(6, right_t, None, twin)
+            go(0, t, 0, right)
+            go(2, t, 1, left)
+            go(1, t, 1, right)
+            go(3, t, 0, left)
+            go(4, t, None, twin)
+
+        def relay():
+            got(0, left_t, 0, left)
+            go(5, left_t, 0, right)
+            got(2, right_t, 1, right)
+            go(6, right_t, 1, left)
+
+        def cross():
+            got(1, left_t, 1, left)
+            go(7, left_t, None, twin)
+            got(3, right_t, 0, right)
+            go(8, right_t, None, twin)
 
         def close():
-            got(3, across_t, 0, left)
-            go(7, across_t, 0, twin)
-            got(5, across_t, 1, right)
-            go(8, across_t, 1, twin)
+            got(5, across_t, 0, left)
+            go(9, across_t, 0, twin)
+            got(6, across_t, 1, right)
+            go(10, across_t, 1, twin)
+            got(4, twin_t, None, twin)
+            got(7, left_t + flip, None, twin)
+            got(8, right_t + flip, None, twin)
 
         def finish():
-            flip = 1 - 2 * c
-            got(2, twin_t, None, twin)
-            got(4, left_t + flip, None, twin)
-            got(6, right_t + flip, None, twin)
-            got(7, across_t + flip, 0, twin)
-            got(8, across_t + flip, 1, twin)
-
-        return start, middle, close, finish
+            got(9, across_t + flip, 0, twin)
+            got(10, across_t + flip, 1, twin)
+
+        return start, relay, cross, close, finish
 
     def tok_view(blk, half):
         r = pl.ds(0, rows) if half is None else pl.ds(half * (rows // 2), rows // 2)
@@ -303,51 +317,65 @@
         cc = pl.ds(0, width) if half is None else pl.ds(half * (width // 2), width // 2)
         return nrm.at[pl.ds(at(blk, block), block), cc]
 
-    def scatter_sum(i, part):
+    rel = (2, 1, 0, 3)
+
+    def scatter_sum(i, blk, bufs, cut, fill_twin, fill_own):
         ss, rs = rs_send.at[i], rs_recv.at[i]
         right, left, twin = {"tp": right_t}, {"tp": left_t}, {"tp": twin_t}
-        hw = width // 2
-
-        for k in (2, 1, 3, 0):
-            xx = lax.rem(x + k, n_x)
-            send(
-                part.at[pl.ds(at(2 * xx + 1 - c, block), block), :],
-                half_recv.at[i, k],
-                ss.at[k],
-                rs.at[k],
-                twin,
-            )
+        pair_in, fwd_in, last_in, fwd_out, last_out = bufs
+        for k in range(n_x):
+            b = 2 * lax.rem(x + rel[k], n_x) + 1 - c
+            fill_twin(b)
+            send(blk(b), pair_in.at[k], ss.at[k], rs.at[k], twin)
 
         def pair(k):
-            arrive(half_recv.at[i, k], ss.at[k], rs.at[k], twin)
-            xx = lax.rem(x + k, n_x)
-            mine = part[pl.ds(at(2 * xx + c, block), block), :]
-            return mine.astype(F32) + half_recv[i, k].astype(F32)
-
-        fwd_send[i] = pair(2).astype(BF)
-        for k, (lo, dev) in enumerate(((0, right), (hw, left))):
-            send(
-                fwd_send.at[i, :, pl.ds(lo, hw)],
-                fwd_recv.at[i, k],
-                ss.at[4 + k],
-                rs.at[4 + k],
-                dev,
-            )
-        s1, s3 = pair(1), pair(3)
-        last_send[i, 0, :, pl.ds(hw, hw)] = s1[:, hw:].astype(BF)
-        last_send[i, 1, :, pl.ds(0, hw)] = s3[:, :hw].astype(BF)
+            b = 2 * lax.rem(x + rel[k], n_x) + c
+            fill_own(b)
+            arrive(pair_in.at[k], ss.at[k], rs.at[k], twin)
+            return blk(b)[...].astype(F32) + pair_in[k].astype(F32)
+
+        def pass_on(src, dst, k, dev):
+            send(src, dst, ss.at[k], rs.at[k], dev)
+
+        s2 = pair(0)
+        fwd_out[...] = s2.astype(BF)
+        pass_on(cut(fwd_out, 0), fwd_in.at[0], 4, right)
+        pass_on(cut(fwd_out, 1), fwd_in.at[1], 5, left)
+        s1 = pair(1)
+        last_out[0] = s1.astype(BF)
+        pass_on(cut(last_out.at[0], 1), cut(last_in.at[0], 1), 6, right)
+        s3 = pair(3)
+        last_out[1] = s3.astype(BF)
+        pass_on(cut(last_out.at[1], 0), cut(last_in.at[1], 0), 7, left)
+        total = pair(2)
         yield
-        arrive(fwd_recv.at[i, 0], ss.at[4], rs.at[4], left)
-        last_send[i, 0, :, pl.ds(0, hw)] = (s1[:, :hw] + fwd_recv[i, 0].astype(F32)).astype(BF)
-        send(last_send.at[i, 0], last_recv.at[i, 0], ss.at[6], rs.at[6], right)
-        arrive(fwd_recv.at[i, 1], ss.at[5], rs.at[5], right)
-        last_send[i, 1, :, pl.ds(hw, hw)] = (s3[:, hw:] + fwd_recv[i, 1].astype(F32)).astype(BF)
-        send(last_send.at[i, 1], last_recv.at[i, 1], ss.at[7], rs.at[7], left)
-        total = pair(0)
+        arrive(fwd_in.at[0], ss.at[4], rs.at[4], left)
+        head = cut(blk(2 * lax.rem(x + 1, n_x) + c), 0)[...].astype(F32)
+        head = head + cut(pair_in.at[1], 0)[...].astype(F32) + fwd_in[0].astype(F32)
+        cut(last_out.at[0], 0)[...] = head.astype(BF)
+        pass_on(cut(last_out.at[0], 0), cut(last_in.at[0], 0), 8, right)
+        arrive(fwd_in.at[1], ss.at[5], rs.at[5], right)
+        head = cut(blk(2 * lax.rem(x + 3, n_x) + c), 1)[...].astype(F32)
+        head = head + cut(pair_in.at[3], 1)[...].astype(F32) + fwd_in[1].astype(F32)
+        cut(last_out.at[1], 1)[...] = head.astype(BF)
+        pass_on(cut(last_out.at[1], 1), cut(last_in.at[1], 1), 9, left)
         yield
-        arrive(last_recv.at[i, 0], ss.at[6], rs.at[6], left)
-        arrive(last_recv.at[i, 1], ss.at[7], rs.at[7], right)
-        yield total + last_recv[i, 0].astype(F32) + last_recv[i, 1].astype(F32)
+        for k, lo, dev in ((6, 0, left), (8, 0, left), (7, 1, right), (9, 1, right)):
+            part = (1 if k == 6 else 0) if lo == 0 else (0 if k == 7 else 1)
+            arrive(cut(last_in.at[lo], part), ss.at[k], rs.at[k], dev)
+        yield total + last_in[0].astype(F32) + last_in[1].astype(F32)
+
+    def row_block(b):
+        return part1.at[pl.ds(at(b, block), block), :]
+
+    def col_block(b):
+        return part2.at[:, pl.ds(at(b, cols), cols)]
+
+    def lane_half(ref, k):
+        return ref.at[:, pl.ds(k * (width // 2), width // 2)]
+
+    def row_half(ref, k):
+        return ref.at[pl.ds(k * (rows // 2), rows // 2), :]
 
     def norm(v, gain):
         mean = jnp.mean(v, axis=1, keepdims=True)
@@ -355,51 +383,46 @@
         var = jnp.mean(d * d, axis=1, keepdims=True)
         return (d * lax.rsqrt(var + EPS) * gain).astype(BF)
 
-    for i in (0, 1, 2):
+    for i in (0, 1, 2, 3):
         moves[i].wait()
-    for d in range(2):
-        z_start(0, d, 1)
-    moves[3].wait()
-    tok_start, tok_middle, tok_close, tok_finish = gather(0, tok_view)
-    tok_start()
+    tok_start, tok_relay, tok_cross, tok_close, tok_finish = gather(0, tok_view)
+    pump(-0.5)
     for i in (4, 5, 6):
         moves[i].wait()
-    for p in (1, 2):
-        for d in range(2):
-            z_start(p, d, 1)
+    pump(0.0)
+    tok_start()
     mine = pl.ds(at(t, cols), cols)
-    for j, (src, dst) in enumerate(((m_gain, mg_all), (o_gain, og_all))):
-        dst[:, mine] = src[...]
-        for k in range(1, n_tp):
-            send(
-                src,
-                dst.at[:, mine],
-                small_send.at[j, k],
-                small_recv.at[j, k],
-                {"tp": lax.rem(t + k, n_tp)},
-            )
-
-    per_hop = 8
-    pump(2 * per_hop)
-    tok_middle()
-    pump(3 * per_hop)
+    mg_all[:, mine] = m_gain[...]
+    for k in range(1, n_tp):
+        send(
+            m_gain,
+            mg_all.at[:, mine],
+            small_send.at[0, k],
+            small_recv.at[0, k],
+            {"tp": lax.rem(t + k, n_tp)},
+        )
+    pump(5.5)
+    tok_relay()
+    pump(8.0)
+    tok_cross()
+    pump(10.8)
     tok_close()
-    pump(4 * per_hop)
+    pump(12.0)
     tok_finish()
 
     key_cols = pl.ds(at(t, DK), DK)
     n_tiles = rows // TILE
     for i in range(n_tiles):
         rr = pl.ds(i * TILE, TILE)
-        low = dot(tok[rr, :], fl[...]).astype(BF)
+        low = dot(tok[rr, :], fl[...], NT).astype(BF)
         pre = dot(low, d_up[:, key_cols]) + d_bias[:, key_cols]
         log_sig = jnp.minimum(pre, 0.0) - jnp.log1p(jnp.exp(-jnp.abs(pre)))
         decay = log_sig / TAU + extra[rr, :]
         hi = decay.astype(BF)
         lo = (decay - hi.astype(F32)).astype(BF)
         esum[i] = jnp.exp(dot(sums[...], jnp.concatenate([hi, lo], axis=0)))
-        pump((5 + i) * per_hop)
-    pump(tail_from)
+        pump(13.0 + i)
+    pump(ATTEND)
     y_done(0)
 
     ii = lax.broadcasted_iota(jnp.int32, (TILE, TILE), 0)
@@ -409,7 +432,6 @@
     for i in range(n_tiles):
         rr = pl.ds(i * TILE, TILE)
         qkv = dot(tok[rr, :], wqkv[...]).astype(BF)
-        ease(4)
         q = qkv[:, :DK].astype(F32) * DK**-0.5
         kb = qkv[:, DK : 2 * DK]
         k = kb.astype(F32)
@@ -429,7 +451,8 @@
             state = state * e_in[TILE - 1 : TILE, :] + fresh
         scale = lax.rsqrt(jnp.mean(got * got, axis=1, keepdims=True) + EPS)
         mixed[rr, :] = (got * scale * h_gain[...]).astype(BF)
-        ease(2)
+        pump(ATTEND + 1.3 * i + 1.0)
+    pump(ATTEND + 5.5)
     y_done(1)
 
     step = 256
@@ -440,32 +463,41 @@
         return 0
 
     lax.fori_loop(0, width // step, mix_cols, 0)
-    rs1 = scatter_sum(0, part1)
+    pump(MIXED)
+
+    def nothing(b):
+        pass
+
+    row_bufs = (pair_row, fwd_row_in, last_row_in, fwd_row_out, last_row_out)
+    rs1 = scatter_sum(0, row_block, row_bufs, lane_half, nothing, nothing)
     next(rs1)
-    ease(6)
+    pump(MIXED + 5.5)
     next(rs1)
-    ease(10)
+    for k in range(1, n_tp):
+        src_t = lax.rem(t + n_tp - k, n_tp)
+        arrive(
+            mg_all.at[:, pl.ds(at(src_t, cols), cols)],
+            small_send.at[0, k],
+            small_recv.at[0, k],
+            {"tp": src_t},
+        )
+    pump(MIXED + 9.5)
     mix = next(rs1)
-    for j, dst in enumerate((mg_all, og_all)):
-        for k in range(1, n_tp):
-            src_t = lax.rem(t + n_tp - k, n_tp)
-            arrive(
-                dst.at[:, pl.ds(at(src_t, cols), cols)],
-                small_send.at[j, k],
-                small_recv.at[j, k],
-                {"tp": src_t},
-            )
     my_rows = pl.ds(at(t, block), block)
     nrm[my_rows, :] = norm(ALPHA * tok[my_rows, :].astype(F32) + mix, mg_all[...])
-    n_start, n_middle, n_close, n_finish = gather(1, nrm_view)
+    n_start, n_relay, n_cross, n_close, n_finish = gather(1, nrm_view)
     n_start()
-    ease(10)
-    n_middle()
-    ease(6)
+    pump(NORMED + 4.5)
+    n_relay()
+    pump(NORMED + 7.0)
+    n_cross()
+    pump(NORMED + 10.0)
     n_close()
+    pump(NORMED + 11.0)
     n_finish()
-    pump(len(order))
+    pump(UP_READY)
     y_done(2)
+    n_up = act.shape[1] // step
 
     def up_cols(j, _):
         cc = pl.ds(pl.multiple_of(j * step, step), step)
@@ -473,39 +505,50 @@
         act[:, cc] = (hidden * hidden).astype(BF)
         return 0
 
-    lax.fori_loop(0, act.shape[1] // step, up_cols, 0)
+    lax.fori_loop(0, n_up // 2, up_cols, 0)
+    pump(UP_READY + 2.0)
+    lax.fori_loop(n_up // 2, n_up, up_cols, 0)
+    pump(1e9)
     y_done(3)
 
-    def down_cols(j, _):
-        cc = pl.ds(pl.multiple_of(j * step, step), step)
+    def down_block(b):
+        cc = pl.ds(at(b, cols), cols)
         part2[:, cc] = dot(act[...], wdn[:, cc]).astype(BF)
-        return 0
-
-    lax.fori_loop(0, width // step, down_cols, 0)
-    rs2 = scatter_sum(1, part2)
+
+    col_bufs = (pair_col, fwd_col_in, last_col_in, fwd_col_out, last_col_out)
+    rs2 = scatter_sum(1, col_block, col_bufs, row_half, down_block, down_block)
     next(rs2)
     next(rs2)
     down = next(rs2)
-    own_out[...] = norm(ALPHA * nrm[my_rows, :].astype(F32) + down, og_all[...])
-    out_buf[my_rows, :] = own_out[:, mine]
+    summed = ALPHA * nrm[:, mine].astype(F32) + down
+
+    ones = jnp.ones((8, cols), BF)
+
+    def row_sums(v):
+        hi = v.astype(BF)
+        lo = (v - hi.astype(F32)).astype(BF)
+        return dot(ones, hi, NT) + dot(ones, lo, NT)
+
+    odd = lax.broadcasted_iota(jnp.int32, (8, rows), 0) % 2 == 1
+    stats[t] = jnp.where(odd, row_sums(summed * summed), row_sums(summed))
     for k in range(1, n_tp):
-        dst_t = lax.rem(t + k, n_tp)
         send(
-            own_out.at[:, pl.ds(at(dst_t, cols), cols)],
-            out_buf.at[my_rows, :],
-            small_send.at[2, k],
-            small_recv.at[2, k],
-            {"tp": dst_t},
+            stats.at[t],
+            stats.at[t],
+            small_send.at[1, k],
+            small_recv.at[1, k],
+            {"tp": lax.rem(t + k, n_tp)},
         )
     for k in range(1, n_tp):
         src_t = lax.rem(t + n_tp - k, n_tp)
-        arrive(
-            out_buf.at[pl.ds(at(src_t, block), block), :],
-            small_send.at[2, k],
-            small_recv.at[2, k],
-            {"tp": src_t},
-        )
-    out[...] = out_buf[...]
+        arrive(stats.at[src_t], small_send.at[1, k], small_recv.at[1, k], {"tp": src_t})
+    both = stats[0]
+    for k in range(1, n_tp):
+        both = both + stats[k]
+    both = jnp.transpose(both) / width
+    mean, square = both[:, 0:1], both[:, 1:2]
+    scale = lax.rsqrt(square - mean * mean + EPS)
+    out[...] = ((summed - mean) * scale * o_gain[...]).astype(BF)
     for copy in pending:
         copy.wait_send()
     for p in range(8):
@@ -562,28 +605,31 @@
                 pltpu.VMEM((rows, vcols), BF),
                 pltpu.VMEM((rows, width), BF),
                 pltpu.VMEM((rows, width), BF),
-                pltpu.VMEM((2, n_tp // 2, block, width), BF),
-                pltpu.VMEM((2, 2, block, width // 2), BF),
-                pltpu.VMEM((2, 2, block, width), BF),
+                pltpu.VMEM((n_tp // 2, block, width), BF),
+                pltpu.VMEM((2, block, width // 2), BF),
                 pltpu.VMEM((2, block, width), BF),
-                pltpu.VMEM((2, 2, block, width), BF),
+                pltpu.VMEM((block, width), BF),
+                pltpu.VMEM((2, block, width), BF),
+                pltpu.VMEM((n_tp // 2, rows, cols), BF),
+                pltpu.VMEM((2, rows // 2, cols), BF),
+                pltpu.VMEM((2, rows, cols), BF),
+                pltpu.VMEM((rows, cols), BF),
+                pltpu.VMEM((2, rows, cols), BF),
                 pltpu.VMEM((rows, width), BF),
                 pltpu.VMEM((rows, hidden), BF),
-                pltpu.VMEM((block, width), BF),
-                pltpu.VMEM((rows, cols), BF),
-                pltpu.VMEM((1, width), F32),
+                pltpu.VMEM((n_tp, 8, rows), F32),
                 pltpu.VMEM((1, width), F32),
                 dma((7,)),
                 dma((8,)),
                 dma((8, 2, far)),
                 dma((4,)),
                 dma((4, n_fs)),
-                dma((2, 9)),
-                dma((2, 9)),
-                dma((2, 8)),
-                dma((2, 8)),
-                dma((3, n_tp)),
-                dma((3, n_tp)),
+                dma((2, 11)),
+                dma((2, 11)),
+                dma((2, 10)),
+                dma((2, 10)),
+                dma((2, n_tp)),
+                dma((2, n_tp)),
             ],
             compiler_params=pltpu.CompilerParams(
                 collective_id=0,
@@ -599,7 +645,7 @@
             out_weight,
             up_weight,
             down_weight,
-            forget_lower_factor,
+            forget_lower_factor.T,
             decay_up,
             decay_bias.reshape(1, -1),
             log_extra,

time: 152 us -> 142 us (0.934)
  Pallas kernels: 148 us -> 140 us
  local copies, waits for them, and re-layouts: 3.57 us -> 1.67 us
    pallas_call x1, Pallas kernels: 148 us -> 140 us  [local(): pl.pallas_call(functools.partial(kernel, n_fs, n_tp), out_shape=jax.Shape...]
    unnamed x2 -> x1, local copies, waits for them, and re-layouts: 3.57 us -> 1.67 us
where the time goes in v2:
time: 142 us
  Pallas kernels  140 us (99%)
  local copies, waits for them, and re-layouts  1.67 us (1%)
    pallas_call x1, Pallas kernels, local(): pl.pallas_call(functools.partial(kernel, n_fs, n_tp), out_shape=jax.Shape...  140 us

profile of v2, /device:TPU:33, one launch (start us, length us, event | category | flops | bytes accessed | tf_op | source)
XLA Modules:
  0.0 141.7 jit_solution(11445657648073082093)
XLA Ops:
  0.0 140.0 %layer.1 = bf16[512,256]{1,0:T(8,128)(2,1)} custom-call(bf16[512,256]{1,0:T(8,128)(2,1)} %tokens.1, bf16[128,128]{1,0:T(8,128)(2,1)} %q_w.1, bf16[128,128]{1,0:T(8,128)(2,1)} %k_w.1, bf16[128,256]{1,0:T(8,128)(2,1)} %v_w.1, bf16[256,128]{1,0:T(8,128)(2,1)} %o_w.1, bf16[128,1024]{1,0:T(8,128)(2,1)} %up_w.1, bf16[1024,128]{1,0:T(8,128)(2,1)} %dn_w.1, ...), custom_call_target="tpu_custom_call" | custom-call | tf_op jit(solution)/shard_map/layer/pallas_call | solution.py:593
  140.1 1.7 %copy.17 = bf16[512,256]{1,0:T(8,128)(2,1)} copy(bf16[512,256]{1,0:T(8,128)(2,1)} %layer.1) | data formatting | bytes 524288

commit v3 on v2

--- a/solution.py
+++ b/solution.py
@@ -40,10 +40,10 @@
 NT = ((1,), (1,))
 TN = ((0,), (0,))
 SIZES = (1.0, 0.5, 1.0, 1.0, 1.0, 1.0, 1.0, 1.0)
-RANKS = (0, 1, 2, 3, 2, 2, 3, 3)
-UNIT, DELAY, LEAD = 1.405, 2.0, 1.0
+BIAS = (-100, -50, 0, 4, 0, 0, 4, 4)
+UNIT, DELAY, LEAD = 1.405, 2.0, (1.0, 3.0)
 RECV, Z_SEND, Y_SEND = 0, 1, 2
-ATTEND, MIXED, NORMED, UP_READY = 31.5, 40.0, 52.0, 64.0
+ATTEND, MIXED, NORMED, UP_READY, DOWN = 31.5, 41.0, 54.0, 70.0, 75.0
 
 
 def ring_plan(reach, shared):
@@ -53,10 +53,10 @@
         free = 0.0
         while waiting:
             now = max(free, min(w[0] for w in waiting))
-            best = min((w for w in waiting if w[0] <= now), key=lambda w: (RANKS[w[1]], w[0]))
+            best = min((w for w in waiting if w[0] <= now), key=lambda w: (w[2] + BIAS[w[1]], w[0]))
             waiting.remove(best)
             since, p, h = best
-            items.append((max(now - LEAD, since), Z_SEND, p, d, h))
+            items.append((max(now - LEAD[now > 30], since), Z_SEND, p, d, h))
             free = now + SIZES[p] * UNIT
             items.append((free + DELAY, RECV, p, d, h))
             if p < shared:
@@ -69,7 +69,7 @@
         best = min((r for r in ready if r[0] <= now), key=lambda r: (r[1], r[0]))
         ready.remove(best)
         since, p, d, h = best
-        items.append((max(now - LEAD, since), Y_SEND, p, d, h))
+        items.append((max(now - LEAD[now > 30], since), Y_SEND, p, d, h))
         free = now + SIZES[p] * UNIT
     return sorted(items)
 
@@ -84,14 +84,14 @@
     o_w,
     up_w,
     dn_w,
-    fl,
-    d_up,
+    fl_in,
+    up_in,
+    extra_in,
+    sums_in,
     d_bias,
-    extra,
     h_gain,
     m_gain,
     o_gain,
-    sums,
     out,
     tok,
     wqkv,
@@ -116,6 +116,10 @@
     act,
     stats,
     mg_all,
+    fl,
+    d_up,
+    extra,
+    sums,
     local_sem,
     z_send,
     z_recv,
@@ -170,6 +174,11 @@
     def arrive(dst, ssem, rsem, dev):
         remote(dst, dst, ssem, rsem, dev).wait_recv()
 
+    barrier = pltpu.get_barrier_semaphore()
+    peers = [{"fs": left_z}, {"fs": right_z}, {"grp": mate}]
+    peers += [{"tp": lax.rem(t + k, n_tp)} for k in range(1, n_tp)]
+    for p in peers:
+        pl.semaphore_signal(barrier, inc=1, device_id=p, device_id_type=MESH)
     my_cols = pl.ds(at(z, zd), zd)
     kw = q_w.shape[1]
     vw = v_w.shape[1]
@@ -182,16 +191,15 @@
         (o_w, wo.at[:, my_cols]),
         (up_w, wup.at[own_rows, :]),
         (dn_w, wdn.at[:, my_cols]),
+        (fl_in, fl),
+        (up_in.at[:, pl.ds(at(t, DK), DK)], d_up),
+        (extra_in, extra),
+        (sums_in, sums),
     ]
     moves = [pltpu.make_async_copy(s, d, local_sem.at[i]) for i, (s, d) in enumerate(moves)]
     for m in moves:
         m.start()
 
-    barrier = pltpu.get_barrier_semaphore()
-    peers = [{"fs": left_z}, {"fs": right_z}, {"grp": mate}]
-    peers += [{"tp": lax.rem(t + k, n_tp)} for k in range(1, n_tp)]
-    for p in peers:
-        pl.semaphore_signal(barrier, inc=1, device_id=p, device_id_type=MESH)
     pl.semaphore_wait(barrier, len(peers))
 
     hq = zd // 2
@@ -246,21 +254,32 @@
         r = region(p, origin(d, h), g)
         remote(r, r, y_send.at[p], y_recv.at[p, y_slot(d, h)], {"grp": mate}).start()
 
+    def y_wait(p, d, h):
+        r = region(p, origin(d, h), 1 - g)
+        arrive(r, y_send.at[p], y_recv.at[p, y_slot(d, h)], {"grp": mate})
+
     def y_done(p):
         for d in range(2):
             for h in range(1, reach[p][d] + 1):
-                r = region(p, origin(d, h), 1 - g)
-                arrive(r, y_send.at[p], y_recv.at[p, y_slot(d, h)], {"grp": mate})
+                y_wait(p, d, h)
 
     steps = {RECV: z_event, Z_SEND: z_start, Y_SEND: y_start}
     order = ring_plan(reach, 4)
     done = [0]
 
+    def take():
+        _, kind, p, d, h = order[done[0]]
+        steps[kind](p, d, h)
+        done[0] += 1
+
+    def pump_hop(pieces, h):
+        need = {(p, d) for p in pieces for d in range(2) if h <= reach[p][d]}
+        while any(o[1] == RECV and o[4] == h and o[2:4] in need for o in order[done[0] :]):
+            take()
+
     def pump(until):
         while done[0] < len(order) and order[done[0]][0] <= until:
-            _, kind, p, d, h = order[done[0]]
-            steps[kind](p, d, h)
-            done[0] += 1
+            take()
 
     def gather(i, view):
         ss, rs = ag_send.at[i], ag_recv.at[i]
@@ -412,10 +431,12 @@
 
     key_cols = pl.ds(at(t, DK), DK)
     n_tiles = rows // TILE
+    for i in range(7, 11):
+        moves[i].wait()
     for i in range(n_tiles):
         rr = pl.ds(i * TILE, TILE)
         low = dot(tok[rr, :], fl[...], NT).astype(BF)
-        pre = dot(low, d_up[:, key_cols]) + d_bias[:, key_cols]
+        pre = dot(low, d_up[...]) + d_bias[:, key_cols]
         log_sig = jnp.minimum(pre, 0.0) - jnp.log1p(jnp.exp(-jnp.abs(pre)))
         decay = log_sig / TAU + extra[rr, :]
         hi = decay.astype(BF)
@@ -495,6 +516,9 @@
     n_close()
     pump(NORMED + 11.0)
     n_finish()
+    for copy in pending:
+        copy.wait_send()
+    pending.clear()
     pump(UP_READY)
     y_done(2)
     n_up = act.shape[1] // step
@@ -506,17 +530,27 @@
         return 0
 
     lax.fori_loop(0, n_up // 2, up_cols, 0)
-    pump(UP_READY + 2.0)
+    pump(UP_READY + 3.0)
     lax.fori_loop(n_up // 2, n_up, up_cols, 0)
+
+    def down_origin(s):
+        cc = pl.ds(at(s, zd), zd)
+        part2[:, cc] = dot(act[...], wdn[:, cc]).astype(BF)
+
+    down_origin(z)
+    for h in range(1, far + 1):
+        pump_hop((3, 6, 7), h)
+        pump(DOWN + 1.4 * h)
+        for d in range(2):
+            if h <= reach[3][d]:
+                y_wait(3, d, h)
+        down_origin(origin(0, h))
+        pump(DOWN + 1.4 * h + 0.7)
+        if h <= near:
+            down_origin(origin(1, h))
     pump(1e9)
-    y_done(3)
-
-    def down_block(b):
-        cc = pl.ds(at(b, cols), cols)
-        part2[:, cc] = dot(act[...], wdn[:, cc]).astype(BF)
-
     col_bufs = (pair_col, fwd_col_in, last_col_in, fwd_col_out, last_col_out)
-    rs2 = scatter_sum(1, col_block, col_bufs, row_half, down_block, down_block)
+    rs2 = scatter_sum(1, col_block, col_bufs, row_half, nothing, nothing)
     next(rs2)
     next(rs2)
     down = next(rs2)
@@ -529,8 +563,8 @@
         lo = (v - hi.astype(F32)).astype(BF)
         return dot(ones, hi, NT) + dot(ones, lo, NT)
 
-    odd = lax.broadcasted_iota(jnp.int32, (8, rows), 0) % 2 == 1
-    stats[t] = jnp.where(odd, row_sums(summed * summed), row_sums(summed))
+    stats[t, :, pl.ds(0, rows)] = row_sums(summed)[0:1, :]
+    stats[t, :, pl.ds(rows, rows)] = row_sums(summed * summed)[0:1, :]
     for k in range(1, n_tp):
         send(
             stats.at[t],
@@ -545,7 +579,8 @@
     both = stats[0]
     for k in range(1, n_tp):
         both = both + stats[k]
-    both = jnp.transpose(both) / width
+    first = lax.broadcasted_iota(jnp.int32, (8, rows), 0) == 0
+    both = jnp.transpose(jnp.where(first, both[:, :rows], both[:, rows:])) / width
     mean, square = both[:, 0:1], both[:, 1:2]
     scale = lax.rsqrt(square - mean * mean + EPS)
     out[...] = ((summed - mean) * scale * o_gain[...]).astype(BF)
@@ -593,7 +628,7 @@
         return pl.pallas_call(
             functools.partial(kernel, n_fs, n_tp),
             out_shape=jax.ShapeDtypeStruct((rows, cols), BF),
-            in_specs=[hbm] * 7 + [vmem] * 8,
+            in_specs=[hbm] * 11 + [vmem] * 4,
             out_specs=vmem,
             scratch_shapes=[
                 pltpu.VMEM((rows, width), BF),
@@ -617,9 +652,13 @@
                 pltpu.VMEM((2, rows, cols), BF),
                 pltpu.VMEM((rows, width), BF),
                 pltpu.VMEM((rows, hidden), BF),
-                pltpu.VMEM((n_tp, 8, rows), F32),
+                pltpu.VMEM((n_tp, 1, 2 * rows), F32),
                 pltpu.VMEM((1, width), F32),
-                dma((7,)),
+                pltpu.VMEM(forget_lower_factor.shape[::-1], BF),
+                pltpu.VMEM((decay_up.shape[0], DK), BF),
+                pltpu.VMEM(log_extra.shape, F32),
+                pltpu.VMEM(sums.shape, BF),
+                dma((11,)),
                 dma((8,)),
                 dma((8, 2, far)),
                 dma((4,)),
@@ -647,12 +686,12 @@
             down_weight,
             forget_lower_factor.T,
             decay_up,
+            log_extra,
+            sums,
             decay_bias.reshape(1, -1),
-            log_extra,
             head_gain.reshape(1, -1),
             mix_gain.reshape(1, -1),
             out_gain.reshape(1, -1),
-            sums,
         )
 
     in_specs = (

time: 142 us -> 137 us (0.965)
  Pallas kernels: 140 us -> 136 us
    pallas_call x1, Pallas kernels: 140 us -> 136 us  [local(): pl.pallas_call(functools.partial(kernel, n_fs, n_tp), out_shape=jax.Shape...]
where the time goes in v3:
time: 137 us
  Pallas kernels  136 us (99%)
  local copies, waits for them, and re-layouts  1.67 us (1%)
    pallas_call x1, Pallas kernels, local(): pl.pallas_call(functools.partial(kernel, n_fs, n_tp), out_shape=jax.Shape...  136 us

profile of v3, /device:TPU:33, one launch (start us, length us, event | category | flops | bytes accessed | tf_op | source)
XLA Modules:
  0.0 137.3 jit_solution(11903173412206015260)
XLA Ops:
  0.0 135.6 %layer.1 = bf16[512,256]{1,0:T(8,128)(2,1)} custom-call(bf16[512,256]{1,0:T(8,128)(2,1)} %tokens.1, bf16[128,128]{1,0:T(8,128)(2,1)} %q_w.1, bf16[128,128]{1,0:T(8,128)(2,1)} %k_w.1, bf16[128,256]{1,0:T(8,128)(2,1)} %v_w.1, bf16[256,128]{1,0:T(8,128)(2,1)} %o_w.1, bf16[128,1024]{1,0:T(8,128)(2,1)} %up_w.1, bf16[1024,128]{1,0:T(8,128)(2,1)} %dn_w.1, ...), custom_call_target="tpu_custom_call" | custom-call | tf_op jit(solution)/shard_map/layer/pallas_call | solution.py:628
  135.6 1.7 %copy.17 = bf16[512,256]{1,0:T(8,128)(2,1)} copy(bf16[512,256]{1,0:T(8,128)(2,1)} %layer.1) | data formatting | bytes 524288

commit v4 on v3

--- a/solution.py
+++ b/solution.py
@@ -164,12 +164,11 @@
             device_id_type=MESH,
         )
 
-    pending = []
-
     def send(src, dst, ssem, rsem, dev):
-        copy = remote(src, dst, ssem, rsem, dev)
-        copy.start()
-        pending.append(copy)
+        remote(src, dst, ssem, rsem, dev).start()
+
+    def sent(amount, ssem, rsem):
+        remote(amount, amount, ssem, rsem, {"tp": twin_t}).wait_send()
 
     def arrive(dst, ssem, rsem, dev):
         remote(dst, dst, ssem, rsem, dev).wait_recv()
@@ -247,21 +246,19 @@
         dev = {"fs": left_z if d == 0 else right_z}
         arrive(region(p, origin(d, h), g), z_send.at[p], z_recv.at[p, d, h - 1], dev)
 
-    def y_slot(d, h):
-        return d * far + h - 1
+    def y_slot(p, h):
+        return p if p < 3 else 2 + h
 
     def y_start(p, d, h):
         r = region(p, origin(d, h), g)
-        remote(r, r, y_send.at[p], y_recv.at[p, y_slot(d, h)], {"grp": mate}).start()
-
-    def y_wait(p, d, h):
-        r = region(p, origin(d, h), 1 - g)
-        arrive(r, y_send.at[p], y_recv.at[p, y_slot(d, h)], {"grp": mate})
+        remote(r, r, y_send.at[p], y_recv.at[y_slot(p, h)], {"grp": mate}).start()
 
     def y_done(p):
-        for d in range(2):
-            for h in range(1, reach[p][d] + 1):
-                y_wait(p, d, h)
+        arrive(whole(p), y_send.at[p], y_recv.at[p], {"grp": mate})
+
+    def y_wait(h):
+        pair = wdn.at[pl.ds(0, hd), pl.ds(0, (2 if h <= near else 1) * zd)]
+        arrive(pair, y_send.at[3], y_recv.at[2 + h], {"grp": mate})
 
     steps = {RECV: z_event, Z_SEND: z_start, Y_SEND: y_start}
     order = ring_plan(reach, 4)
@@ -282,30 +279,29 @@
             take()
 
     def gather(i, view):
-        ss, rs = ag_send.at[i], ag_recv.at[i]
+        ss = ag_send.at[i]
+        rs = ag_recv.at[i]
         right, left, twin = {"tp": right_t}, {"tp": left_t}, {"tp": twin_t}
 
         def go(k, blk, half, dev):
             v = view(blk, half)
-            send(v, v, ss.at[k], rs.at[k], dev)
+            send(v, v, ss, rs.at[min(k, 6)], dev)
 
         def got(k, blk, half, dev):
-            arrive(view(blk, half), ss.at[k], rs.at[k], dev)
-
-        flip = 1 - 2 * c
+            arrive(view(blk, half), ss, rs.at[k], dev)
 
         def start():
             go(0, t, 0, right)
             go(2, t, 1, left)
             go(1, t, 1, right)
             go(3, t, 0, left)
-            go(4, t, None, twin)
+            go(6, t, None, twin)
 
         def relay():
             got(0, left_t, 0, left)
-            go(5, left_t, 0, right)
+            go(4, left_t, 0, right)
             got(2, right_t, 1, right)
-            go(6, right_t, 1, left)
+            go(5, right_t, 1, left)
 
         def cross():
             got(1, left_t, 1, left)
@@ -314,17 +310,13 @@
             go(8, right_t, None, twin)
 
         def close():
-            got(5, across_t, 0, left)
+            got(4, across_t, 0, left)
             go(9, across_t, 0, twin)
-            got(6, across_t, 1, right)
+            got(5, across_t, 1, right)
             go(10, across_t, 1, twin)
-            got(4, twin_t, None, twin)
-            got(7, left_t + flip, None, twin)
-            got(8, right_t + flip, None, twin)
 
         def finish():
-            got(9, across_t + flip, 0, twin)
-            got(10, across_t + flip, 1, twin)
+            arrive(tok.at[:, pl.ds(0, n_x * cols)], ss, rs.at[6], twin)
 
         return start, relay, cross, close, finish
 
@@ -339,22 +331,23 @@
     rel = (2, 1, 0, 3)
 
     def scatter_sum(i, blk, bufs, cut, fill_twin, fill_own):
-        ss, rs = rs_send.at[i], rs_recv.at[i]
+        ss = rs_send.at[i]
+        rs = rs_recv.at[i]
         right, left, twin = {"tp": right_t}, {"tp": left_t}, {"tp": twin_t}
         pair_in, fwd_in, last_in, fwd_out, last_out = bufs
         for k in range(n_x):
             b = 2 * lax.rem(x + rel[k], n_x) + 1 - c
             fill_twin(b)
-            send(blk(b), pair_in.at[k], ss.at[k], rs.at[k], twin)
+            send(blk(b), pair_in.at[k], ss, rs.at[k], twin)
 
         def pair(k):
             b = 2 * lax.rem(x + rel[k], n_x) + c
             fill_own(b)
-            arrive(pair_in.at[k], ss.at[k], rs.at[k], twin)
+            arrive(pair_in.at[k], ss, rs.at[k], twin)
             return blk(b)[...].astype(F32) + pair_in[k].astype(F32)
 
         def pass_on(src, dst, k, dev):
-            send(src, dst, ss.at[k], rs.at[k], dev)
+            send(src, dst, ss, rs.at[min(k, 6)], dev)
 
         s2 = pair(0)
         fwd_out[...] = s2.astype(BF)
@@ -368,20 +361,18 @@
         pass_on(cut(last_out.at[1], 0), cut(last_in.at[1], 0), 7, left)
         total = pair(2)
         yield
-        arrive(fwd_in.at[0], ss.at[4], rs.at[4], left)
+        arrive(fwd_in.at[0], ss, rs.at[4], left)
         head = cut(blk(2 * lax.rem(x + 1, n_x) + c), 0)[...].astype(F32)
         head = head + cut(pair_in.at[1], 0)[...].astype(F32) + fwd_in[0].astype(F32)
         cut(last_out.at[0], 0)[...] = head.astype(BF)
         pass_on(cut(last_out.at[0], 0), cut(last_in.at[0], 0), 8, right)
-        arrive(fwd_in.at[1], ss.at[5], rs.at[5], right)
+        arrive(fwd_in.at[1], ss, rs.at[5], right)
         head = cut(blk(2 * lax.rem(x + 3, n_x) + c), 1)[...].astype(F32)
         head = head + cut(pair_in.at[3], 1)[...].astype(F32) + fwd_in[1].astype(F32)
         cut(last_out.at[1], 1)[...] = head.astype(BF)
         pass_on(cut(last_out.at[1], 1), cut(last_in.at[1], 1), 9, left)
         yield
-        for k, lo, dev in ((6, 0, left), (8, 0, left), (7, 1, right), (9, 1, right)):
-            part = (1 if k == 6 else 0) if lo == 0 else (0 if k == 7 else 1)
-            arrive(cut(last_in.at[lo], part), ss.at[k], rs.at[k], dev)
+        arrive(last_in, ss, rs.at[6], left)
         yield total + last_in[0].astype(F32) + last_in[1].astype(F32)
 
     def row_block(b):
@@ -416,8 +407,8 @@
         send(
             m_gain,
             mg_all.at[:, mine],
-            small_send.at[0, k],
-            small_recv.at[0, k],
+            small_send.at[0],
+            small_recv.at[0],
             {"tp": lax.rem(t + k, n_tp)},
         )
     pump(5.5)
@@ -494,14 +485,8 @@
     next(rs1)
     pump(MIXED + 5.5)
     next(rs1)
-    for k in range(1, n_tp):
-        src_t = lax.rem(t + n_tp - k, n_tp)
-        arrive(
-            mg_all.at[:, pl.ds(at(src_t, cols), cols)],
-            small_send.at[0, k],
-            small_recv.at[0, k],
-            {"tp": src_t},
-        )
+    gains = mg_all.at[:, pl.ds(0, (n_tp - 1) * cols)]
+    arrive(gains, small_send.at[0], small_recv.at[0], {"tp": twin_t})
     pump(MIXED + 9.5)
     mix = next(rs1)
     my_rows = pl.ds(at(t, block), block)
@@ -516,9 +501,11 @@
     n_close()
     pump(NORMED + 11.0)
     n_finish()
-    for copy in pending:
-        copy.wait_send()
-    pending.clear()
+    most = pl.ds(0, (n_tp - 1) * cols)
+    for i in range(2):
+        sent(tok.at[:, most], ag_send.at[i], ag_recv.at[i, 0])
+    sent(tok.at[:, most], rs_send.at[0], rs_recv.at[0, 0])
+    sent(gains, small_send.at[0], small_recv.at[0])
     pump(UP_READY)
     y_done(2)
     n_up = act.shape[1] // step
@@ -541,9 +528,7 @@
     for h in range(1, far + 1):
         pump_hop((3, 6, 7), h)
         pump(DOWN + 1.4 * h)
-        for d in range(2):
-            if h <= reach[3][d]:
-                y_wait(3, d, h)
+        y_wait(h)
         down_origin(origin(0, h))
         pump(DOWN + 1.4 * h + 0.7)
         if h <= near:
@@ -569,13 +554,12 @@
         send(
             stats.at[t],
             stats.at[t],
-            small_send.at[1, k],
-            small_recv.at[1, k],
+            small_send.at[1],
+            small_recv.at[1],
             {"tp": lax.rem(t + k, n_tp)},
         )
-    for k in range(1, n_tp):
-        src_t = lax.rem(t + n_tp - k, n_tp)
-        arrive(stats.at[src_t], small_send.at[1, k], small_recv.at[1, k], {"tp": src_t})
+    others = stats.at[pl.ds(0, n_tp - 1)]
+    arrive(others, small_send.at[1], small_recv.at[1], {"tp": twin_t})
     both = stats[0]
     for k in range(1, n_tp):
         both = both + stats[k]
@@ -584,13 +568,13 @@
     mean, square = both[:, 0:1], both[:, 1:2]
     scale = lax.rsqrt(square - mean * mean + EPS)
     out[...] = ((summed - mean) * scale * o_gain[...]).astype(BF)
-    for copy in pending:
-        copy.wait_send()
+    sent(tok.at[:, most], rs_send.at[1], rs_recv.at[1, 0])
+    sent(others, small_send.at[1], small_recv.at[1])
     for p in range(8):
         w = whole(p)
         remote(w, w, z_send.at[p], z_recv.at[p, 0, 0], {"fs": right_z}).wait_send()
         if p < 4:
-            remote(w, w, y_send.at[p], y_recv.at[p, 0], {"grp": mate}).wait_send()
+            remote(w, w, y_send.at[p], y_recv.at[p], {"grp": mate}).wait_send()
 
 
 def solution(mesh):
@@ -662,13 +646,13 @@
                 dma((8,)),
                 dma((8, 2, far)),
                 dma((4,)),
-                dma((4, n_fs)),
-                dma((2, 11)),
-                dma((2, 11)),
-                dma((2, 10)),
-                dma((2, 10)),
-                dma((2, n_tp)),
-                dma((2, n_tp)),
+                dma((3 + far,)),
+                dma((2,)),
+                dma((2, 7)),
+                dma((2,)),
+                dma((2, 7)),
+                dma((2,)),
+                dma((2,)),
             ],
             compiler_params=pltpu.CompilerParams(
                 collective_id=0,

time: 137 us -> 136 us (level)
  Pallas kernels: 136 us -> 134 us
where the time goes in v4:
time: 136 us
  Pallas kernels  134 us (99%)
  local copies, waits for them, and re-layouts  1.67 us (1%)
    pallas_call x1, Pallas kernels, local(): pl.pallas_call(functools.partial(kernel, n_fs, n_tp), out_shape=jax.Shape...  134 us

profile of v4, /device:TPU:33, one launch (start us, length us, event | category | flops | bytes accessed | tf_op | source)
XLA Modules:
  0.0 135.9 jit_solution(9798794898579614778)
XLA Ops:
  0.0 134.3 %layer.1 = bf16[512,256]{1,0:T(8,128)(2,1)} custom-call(bf16[512,256]{1,0:T(8,128)(2,1)} %tokens.1, bf16[128,128]{1,0:T(8,128)(2,1)} %q_w.1, bf16[128,128]{1,0:T(8,128)(2,1)} %k_w.1, bf16[128,256]{1,0:T(8,128)(2,1)} %v_w.1, bf16[256,128]{1,0:T(8,128)(2,1)} %o_w.1, bf16[128,1024]{1,0:T(8,128)(2,1)} %up_w.1, bf16[1024,128]{1,0:T(8,128)(2,1)} %dn_w.1, ...), custom_call_target="tpu_custom_call" | custom-call | tf_op jit(solution)/shard_map/layer/pallas_call | solution.py:612
  134.3 1.7 %copy.17 = bf16[512,256]{1,0:T(8,128)(2,1)} copy(bf16[512,256]{1,0:T(8,128)(2,1)} %layer.1) | data formatting | bytes 524288

commit v5 on v4

--- a/solution.py
+++ b/solution.py
@@ -330,21 +330,18 @@
 
     rel = (2, 1, 0, 3)
 
-    def scatter_sum(i, blk, bufs, cut, fill_twin, fill_own):
+    def scatter_sum(i, blk, bufs, cut, pair_at, collect):
         ss = rs_send.at[i]
         rs = rs_recv.at[i]
         right, left, twin = {"tp": right_t}, {"tp": left_t}, {"tp": twin_t}
-        pair_in, fwd_in, last_in, fwd_out, last_out = bufs
-        for k in range(n_x):
-            b = 2 * lax.rem(x + rel[k], n_x) + 1 - c
-            fill_twin(b)
-            send(blk(b), pair_in.at[k], ss, rs.at[k], twin)
+        fwd_in, last_in, fwd_out, last_out = bufs
+
+        def mine_at(k):
+            return 2 * lax.rem(x + rel[k], n_x) + c
 
         def pair(k):
-            b = 2 * lax.rem(x + rel[k], n_x) + c
-            fill_own(b)
-            arrive(pair_in.at[k], ss, rs.at[k], twin)
-            return blk(b)[...].astype(F32) + pair_in[k].astype(F32)
+            collect(k)
+            return blk(mine_at(k))[...].astype(F32) + pair_at(k)[...].astype(F32)
 
         def pass_on(src, dst, k, dev):
             send(src, dst, ss, rs.at[min(k, 6)], dev)
@@ -362,13 +359,13 @@
         total = pair(2)
         yield
         arrive(fwd_in.at[0], ss, rs.at[4], left)
-        head = cut(blk(2 * lax.rem(x + 1, n_x) + c), 0)[...].astype(F32)
-        head = head + cut(pair_in.at[1], 0)[...].astype(F32) + fwd_in[0].astype(F32)
+        head = cut(blk(mine_at(1)), 0)[...].astype(F32)
+        head = head + cut(pair_at(1), 0)[...].astype(F32) + fwd_in[0].astype(F32)
         cut(last_out.at[0], 0)[...] = head.astype(BF)
         pass_on(cut(last_out.at[0], 0), cut(last_in.at[0], 0), 8, right)
         arrive(fwd_in.at[1], ss, rs.at[5], right)
-        head = cut(blk(2 * lax.rem(x + 3, n_x) + c), 1)[...].astype(F32)
-        head = head + cut(pair_in.at[3], 1)[...].astype(F32) + fwd_in[1].astype(F32)
+        head = cut(blk(mine_at(3)), 1)[...].astype(F32)
+        head = head + cut(pair_at(3), 1)[...].astype(F32) + fwd_in[1].astype(F32)
         cut(last_out.at[1], 1)[...] = head.astype(BF)
         pass_on(cut(last_out.at[1], 1), cut(last_in.at[1], 1), 9, left)
         yield
@@ -477,11 +474,18 @@
     lax.fori_loop(0, width // step, mix_cols, 0)
     pump(MIXED)
 
-    def nothing(b):
-        pass
-
-    row_bufs = (pair_row, fwd_row_in, last_row_in, fwd_row_out, last_row_out)
-    rs1 = scatter_sum(0, row_block, row_bufs, lane_half, nothing, nothing)
+    for k in range(n_x):
+        b = 2 * lax.rem(x + rel[k], n_x) + 1 - c
+        send(row_block(b), pair_row.at[k], rs_send.at[0], rs_recv.at[0, k], {"tp": twin_t})
+
+    def row_pair(k):
+        return pair_row.at[k]
+
+    def row_collect(k):
+        arrive(pair_row.at[k], rs_send.at[0], rs_recv.at[0, k], {"tp": twin_t})
+
+    row_bufs = (fwd_row_in, last_row_in, fwd_row_out, last_row_out)
+    rs1 = scatter_sum(0, row_block, row_bufs, lane_half, row_pair, row_collect)
     next(rs1)
     pump(MIXED + 5.5)
     next(rs1)
@@ -524,6 +528,10 @@
         cc = pl.ds(at(s, zd), zd)
         part2[:, cc] = dot(act[...], wdn[:, cc]).astype(BF)
 
+        @pl.when(lax.rem(s // (cols // zd), 2) != c)
+        def _():
+            send(part2.at[:, cc], pair_col.at[:, cc], rs_send.at[1], rs_recv.at[1, 0], {"tp": twin_t})
+
     down_origin(z)
     for h in range(1, far + 1):
         pump_hop((3, 6, 7), h)
@@ -534,8 +542,17 @@
         if h <= near:
             down_origin(origin(1, h))
     pump(1e9)
-    col_bufs = (pair_col, fwd_col_in, last_col_in, fwd_col_out, last_col_out)
-    rs2 = scatter_sum(1, col_block, col_bufs, row_half, nothing, nothing)
+
+    def col_pair(k):
+        return pair_col.at[:, pl.ds(at(2 * lax.rem(x + rel[k], n_x) + c, cols), cols)]
+
+    def col_collect(k):
+        if k == 0:
+            half = pair_col.at[:, pl.ds(0, n_x * cols)]
+            arrive(half, rs_send.at[1], rs_recv.at[1, 0], {"tp": twin_t})
+
+    col_bufs = (fwd_col_in, last_col_in, fwd_col_out, last_col_out)
+    rs2 = scatter_sum(1, col_block, col_bufs, row_half, col_pair, col_collect)
     next(rs2)
     next(rs2)
     down = next(rs2)
@@ -629,7 +646,7 @@
                 pltpu.VMEM((2, block, width), BF),
                 pltpu.VMEM((block, width), BF),
                 pltpu.VMEM((2, block, width), BF),
-                pltpu.VMEM((n_tp // 2, rows, cols), BF),
+                pltpu.VMEM((rows, width), BF),
                 pltpu.VMEM((2, rows // 2, cols), BF),
                 pltpu.VMEM((2, rows, cols), BF),
                 pltpu.VMEM((rows, cols), BF),

time: 136 us -> 139 us (1.022)
  Pallas kernels: 134 us -> 137 us
    pallas_call x1, Pallas kernels: 134 us -> 137 us  [local(): pl.pallas_call(functools.partial(kernel, n_fs, n_tp), out_shape=jax.Shape...]
where the time goes in v5:
time: 139 us; the launch traced here: 138 us
  Pallas kernels  137 us (99%)
  local copies, waits for them, and re-layouts  1.67 us (1%)
    pallas_call x1, Pallas kernels, local(): pl.pallas_call(functools.partial(kernel, n_fs, n_tp), out_shape=jax.Shape...  137 us

profile of v5, /device:TPU:33, one launch (start us, length us, event | category | flops | bytes accessed | tf_op | source)
XLA Modules:
  0.0 138.4 jit_solution(1186400388026632821)
XLA Ops:
  0.0 136.8 %layer.1 = bf16[512,256]{1,0:T(8,128)(2,1)} custom-call(bf16[512,256]{1,0:T(8,128)(2,1)} %tokens.1, bf16[128,128]{1,0:T(8,128)(2,1)} %q_w.1, bf16[128,128]{1,0:T(8,128)(2,1)} %k_w.1, bf16[128,256]{1,0:T(8,128)(2,1)} %v_w.1, bf16[256,128]{1,0:T(8,128)(2,1)} %o_w.1, bf16[128,1024]{1,0:T(8,128)(2,1)} %up_w.1, bf16[1024,128]{1,0:T(8,128)(2,1)} %dn_w.1, ...), custom_call_target="tpu_custom_call" | custom-call | tf_op jit(solution)/shard_map/layer/pallas_call | solution.py:629
  136.8 1.7 %copy.17 = bf16[512,256]{1,0:T(8,128)(2,1)} copy(bf16[512,256]{1,0:T(8,128)(2,1)} %layer.1) | data formatting | bytes 524288

commit v6 on v4

--- a/solution.py
+++ b/solution.py
@@ -40,10 +40,10 @@
 NT = ((1,), (1,))
 TN = ((0,), (0,))
 SIZES = (1.0, 0.5, 1.0, 1.0, 1.0, 1.0, 1.0, 1.0)
-BIAS = (-100, -50, 0, 4, 0, 0, 4, 4)
-UNIT, DELAY, LEAD = 1.405, 2.0, (1.0, 3.0)
+BIAS = (-100, -3, 0, 5, 0, 0, 5, 5)
+UNIT, DELAY, LEAD = 1.405, 2.9, 2.0
 RECV, Z_SEND, Y_SEND = 0, 1, 2
-ATTEND, MIXED, NORMED, UP_READY, DOWN = 31.5, 41.0, 54.0, 70.0, 75.0
+ATTEND, MIXED, NORMED, UP_READY, DOWN = 41.8, 50.2, 59.6, 70.0, 74.0
 
 
 def ring_plan(reach, shared):
@@ -56,7 +56,7 @@
             best = min((w for w in waiting if w[0] <= now), key=lambda w: (w[2] + BIAS[w[1]], w[0]))
             waiting.remove(best)
             since, p, h = best
-            items.append((max(now - LEAD[now > 30], since), Z_SEND, p, d, h))
+            items.append((max(now - LEAD, since), Z_SEND, p, d, h))
             free = now + SIZES[p] * UNIT
             items.append((free + DELAY, RECV, p, d, h))
             if p < shared:
@@ -69,7 +69,7 @@
         best = min((r for r in ready if r[0] <= now), key=lambda r: (r[1], r[0]))
         ready.remove(best)
         since, p, d, h = best
-        items.append((max(now - LEAD[now > 30], since), Y_SEND, p, d, h))
+        items.append((max(now - LEAD, since), Y_SEND, p, d, h))
         free = now + SIZES[p] * UNIT
     return sorted(items)
 
@@ -516,23 +516,21 @@
         act[:, cc] = (hidden * hidden).astype(BF)
         return 0
 
+    hops = [0]
     lax.fori_loop(0, n_up // 2, up_cols, 0)
     pump(UP_READY + 3.0)
     lax.fori_loop(n_up // 2, n_up, up_cols, 0)
 
-    def down_origin(s):
-        cc = pl.ds(at(s, zd), zd)
+    n_pairs = n_fs // 2
+    for i, h in [(0, 1)] + [(k, min(2 * abs(k) + 1, far)) for m in range(1, far // 2) for k in (m, -m)] + [(far // 2, far)]:
+        while hops[0] < h:
+            hops[0] += 1
+            pump_hop((3, 6, 7), hops[0])
+            y_wait(hops[0])
+        pump(DOWN + 1.2 * h)
+        pair_at = lax.rem(z // 2 + i + n_pairs, n_pairs)
+        cc = pl.ds(at(pair_at, 2 * zd), 2 * zd)
         part2[:, cc] = dot(act[...], wdn[:, cc]).astype(BF)
-
-    down_origin(z)
-    for h in range(1, far + 1):
-        pump_hop((3, 6, 7), h)
-        pump(DOWN + 1.4 * h)
-        y_wait(h)
-        down_origin(origin(0, h))
-        pump(DOWN + 1.4 * h + 0.7)
-        if h <= near:
-            down_origin(origin(1, h))
     pump(1e9)
     col_bufs = (pair_col, fwd_col_in, last_col_in, fwd_col_out, last_col_out)
     rs2 = scatter_sum(1, col_block, col_bufs, row_half, nothing, nothing)

time: 136 us -> 135 us (level)
  no operation moved by 1% of the time
where the time goes in v6:
time: 135 us
  Pallas kernels  134 us (99%)
  local copies, waits for them, and re-layouts  1.67 us (1%)
    pallas_call x1, Pallas kernels, local(): pl.pallas_call(functools.partial(kernel, n_fs, n_tp), out_shape=jax.Shape...  134 us

profile of v6, /device:TPU:33, one launch (start us, length us, event | category | flops | bytes accessed | tf_op | source)
XLA Modules:
  0.0 135.3 jit_solution(6359019962280018557)
XLA Ops:
  0.0 133.6 %layer.1 = bf16[512,256]{1,0:T(8,128)(2,1)} custom-call(bf16[512,256]{1,0:T(8,128)(2,1)} %tokens.1, bf16[128,128]{1,0:T(8,128)(2,1)} %q_w.1, bf16[128,128]{1,0:T(8,128)(2,1)} %k_w.1, bf16[128,256]{1,0:T(8,128)(2,1)} %v_w.1, bf16[256,128]{1,0:T(8,128)(2,1)} %o_w.1, bf16[128,1024]{1,0:T(8,128)(2,1)} %up_w.1, bf16[1024,128]{1,0:T(8,128)(2,1)} %dn_w.1, ...), custom_call_target="tpu_custom_call" | custom-call | tf_op jit(solution)/shard_map/layer/pallas_call | solution.py:610
  133.7 1.7 %copy.17 = bf16[512,256]{1,0:T(8,128)(2,1)} copy(bf16[512,256]{1,0:T(8,128)(2,1)} %layer.1) | data formatting | bytes 524288

commit v7 on v6

--- a/solution.py
+++ b/solution.py
@@ -43,7 +43,7 @@
 BIAS = (-100, -3, 0, 5, 0, 0, 5, 5)
 UNIT, DELAY, LEAD = 1.405, 2.9, 2.0
 RECV, Z_SEND, Y_SEND = 0, 1, 2
-ATTEND, MIXED, NORMED, UP_READY, DOWN = 41.8, 50.2, 59.6, 70.0, 74.0
+ATTEND, MIXED, NORMED, UP_READY, DOWN = 41.8, 51.0, 63.0, 76.0, 80.0
 
 
 def ring_plan(reach, shared):
@@ -463,8 +463,8 @@
             state = state * e_in[TILE - 1 : TILE, :] + fresh
         scale = lax.rsqrt(jnp.mean(got * got, axis=1, keepdims=True) + EPS)
         mixed[rr, :] = (got * scale * h_gain[...]).astype(BF)
-        pump(ATTEND + 1.3 * i + 1.0)
-    pump(ATTEND + 5.5)
+        pump(ATTEND + 1.3 * i + 2.0)
+    pump(ATTEND + 6.5)
     y_done(1)
 
     step = 256
@@ -483,11 +483,11 @@
     row_bufs = (pair_row, fwd_row_in, last_row_in, fwd_row_out, last_row_out)
     rs1 = scatter_sum(0, row_block, row_bufs, lane_half, nothing, nothing)
     next(rs1)
-    pump(MIXED + 5.5)
+    pump(MIXED + 7.0)
     next(rs1)
     gains = mg_all.at[:, pl.ds(0, (n_tp - 1) * cols)]
     arrive(gains, small_send.at[0], small_recv.at[0], {"tp": twin_t})
-    pump(MIXED + 9.5)
+    pump(MIXED + 11.5)
     mix = next(rs1)
     my_rows = pl.ds(at(t, block), block)
     nrm[my_rows, :] = norm(ALPHA * tok[my_rows, :].astype(F32) + mix, mg_all[...])

time: 135 us -> 133 us (0.985)
  Pallas kernels: 134 us -> 132 us
    pallas_call x1, Pallas kernels: 134 us -> 132 us  [local(): pl.pallas_call(functools.partial(kernel, n_fs, n_tp), out_shape=jax.Shape...]
where the time goes in v7:
time: 133 us
  Pallas kernels  132 us (99%)
  local copies, waits for them, and re-layouts  1.67 us (1%)
    pallas_call x1, Pallas kernels, local(): pl.pallas_call(functools.partial(kernel, n_fs, n_tp), out_shape=jax.Shape...  132 us

profile of v7, /device:TPU:33, one launch (start us, length us, event | category | flops | bytes accessed | tf_op | source)
XLA Modules:
  0.0 133.3 jit_solution(11063371571044427511)
XLA Ops:
  0.0 131.6 %layer.1 = bf16[512,256]{1,0:T(8,128)(2,1)} custom-call(bf16[512,256]{1,0:T(8,128)(2,1)} %tokens.1, bf16[128,128]{1,0:T(8,128)(2,1)} %q_w.1, bf16[128,128]{1,0:T(8,128)(2,1)} %k_w.1, bf16[128,256]{1,0:T(8,128)(2,1)} %v_w.1, bf16[256,128]{1,0:T(8,128)(2,1)} %o_w.1, bf16[128,1024]{1,0:T(8,128)(2,1)} %up_w.1, bf16[1024,128]{1,0:T(8,128)(2,1)} %dn_w.1, ...), custom_call_target="tpu_custom_call" | custom-call | tf_op jit(solution)/shard_map/layer/pallas_call | solution.py:610
  131.6 1.7 %copy.17 = bf16[512,256]{1,0:T(8,128)(2,1)} copy(bf16[512,256]{1,0:T(8,128)(2,1)} %layer.1) | data formatting | bytes 524288
